TPU v7x, 32 devices: a whole 2x2x4 slice. The times are simulated.
32 devices in a mesh: sp: 8 (over z, y), tp: 4 (over x, core).
Axes of the slice: x: 2, y: 2, z: 4, core: 2. Of those that a mesh axis runs over, the one named last changes fastest.
Arguments:
- tokens: bfloat16 [1536, 2048], P(('sp', 'tp')), may hold values from -6 to 6
- norm_in: float32 [2048], replicated, may hold values from 0.1 to 1.9
- decay_log: float32 [128, 64], P('tp'), may hold values from -0.034 to -0.00016276042, as said below
- phase: float32 [128, 64], P('tp'), may hold values from -1 to 1
- b_real: float32 [128, 64, 16], P('tp'), may hold values from -1 to 1
- b_imag: float32 [128, 64, 16], P('tp'), may hold values from -1 to 1
- c_real: float32 [128, 16, 64], P('tp'), may hold values from -0.75 to 0.75
- c_imag: float32 [128, 16, 64], P('tp'), may hold values from -0.75 to 0.75
- skip_gain: float32 [2048], P('tp'), may hold values from -6 to 6
- w_value: bfloat16 [2048, 2048], P(None, 'tp'), as said below
- w_gate: bfloat16 [2048, 2048], P(None, 'tp'), may hold values from -0.125 to 0.125
- norm_out: float32 [2048], P('tp'), may hold values from 0.1 to 1.9
Outputs:
- mixed: bfloat16 [1536, 2048], P('sp', 'tp')
Inputs may be any that keep to these rules, and one draw needn't show every extreme that they name: `decay_log`: negative real parts of the eigenvalues. `w_value`: weights of the value projection.
All inputs are finite; a program needn't handle non-finite values.
Results may differ from a plain program's by a relative error of at most 0.012.
The roundings to bfloat16 on the way count: a program that leaves them out, or rounds other values in their place, can miss the bound.
Values may be sent and summed in bfloat16 or wider, within the bound.
A program may use at most 64 MiB of HBM per device.

v0:
```python
import functools

import jax
import jax.numpy as jnp
from jax import lax
from jax.experimental import pallas as pl
from jax.experimental.pallas import tpu as pltpu
from jax.sharding import PartitionSpec as P

NORM_EPS = 1e-06
LANES = 128
F32 = jnp.float32
BF16 = jnp.bfloat16
NT = (((1,), (1,)), ((), ()))


def cmul(ar, ai, br, bi):
    return ar * br - ai * bi, ar * bi + ai * br


def exact(ones, value):
    total = None
    for _ in range(3):
        term = value.astype(BF16)
        value = value - term.astype(F32)
        dot = lax.dot_general(ones, term, NT, preferred_element_type=F32)
        total = dot if total is None else total + dot
    return total


def remote(src, dst, send, recv, target):
    return pltpu.make_async_remote_copy(
        src_ref=src,
        dst_ref=dst,
        send_sem=send,
        recv_sem=recv,
        device_id=target,
        device_id_type=pl.DeviceIdType.MESH,
    )


def layer(
    n_sp, n_tp, state, group,
    tok_h, nin_h, dlog_h, phase_h, bre_h, bim_h, cre_h, cim_h, skip_h, wv_h, wg_h, nout_h,
    out,
    nsend, urecv, uf, rows_a, rows_p, t1r, t1i, t2r, t2i, bs, cs, wbuf, ylocal,
    e_send, e_all, l_ref, zbuf, wv, wg, acc_v, acc_g, sq_all,
    bre, bim, cre, cim, tok, nin, dlog, phase, skip, nout,
    load_sem, a_send, a_recv, e_ssem, e_rsem, z_send, z_recv, f_send, q_send, q_recv, met,
):
    sp, tp = lax.axis_index("sp"), lax.axis_index("tp")
    mine, d_model = tok.shape
    rows, width = uf.shape
    n_blk = width // LANES
    per = LANES // group
    lanes = per * state
    core = lax.rem(tp, 2)
    partner = tp + 1 - 2 * core
    n_chip = n_tp // 2

    loads = [
        pltpu.make_async_copy(src, dst, load_sem.at[i])
        for i, (src, dst) in enumerate(
            (
                (tok_h, tok), (nin_h, nin), (dlog_h, dlog), (phase_h, phase),
                (bre_h, bre), (bim_h, bim), (cre_h, cre), (cim_h, cim),
                (skip_h, skip), (nout_h, nout), (wv_h, wv), (wg_h, wg),
            )
        )
    ]
    for copy in loads[:4]:
        copy.start()

    barrier = pltpu.get_barrier_semaphore()

    def signal_sp(sem, d):
        for ok, to in ((sp >= d, sp - d), (sp + d < n_sp, sp + d)):

            @pl.when(ok)
            def _(to=to):
                pl.semaphore_signal(
                    sem, inc=1, device_id={"sp": to}, device_id_type=pl.DeviceIdType.MESH
                )

    def around(d):
        return jnp.where(sp >= d, 1, 0) + jnp.where(sp + d < n_sp, 1, 0)

    signal_sp(barrier, 1)
    for k in range(1, n_tp):
        pl.semaphore_signal(
            barrier, inc=1, device_id={"tp": lax.rem(tp + k, n_tp)},
            device_id_type=pl.DeviceIdType.MESH,
        )
    for copy in loads[4:10]:
        copy.start()
    for copy in loads[:4]:
        copy.wait()

    xf = tok[...].astype(F32)
    scale = lax.rsqrt(jnp.sum(xf * xf, axis=1, keepdims=True) / d_model + NORM_EPS)
    normed = (xf * scale * nin[...]).astype(BF16)
    for j in range(n_tp):
        for blk in range(n_blk):
            at = j * width + blk * LANES
            nsend[j, blk] = normed[:, at : at + LANES]

    side = LANES // state
    for i in range(width // group // side):
        cut = slice(i * LANES, (i + 1) * LANES)
        for src, dst in ((dlog, rows_a), (phase, rows_p)):
            row = jnp.concatenate([src[i * side + k : i * side + k + 1, :] for k in range(side)], axis=1)
            dst[:, cut] = jnp.broadcast_to(row, (8, LANES))

    for blk in range(n_blk):
        cut = slice(blk * lanes, (blk + 1) * lanes)
        a, p = rows_a[:, cut], rows_p[:, cut]
        k = lax.broadcasted_iota(jnp.int32, a.shape, 0).astype(F32)
        mag, cos, sin = jnp.exp(a), jnp.cos(p), jnp.sin(p)
        lr, li = mag * cos, mag * sin
        inv = jnp.exp(-a)
        nr, ni = inv * cos, -inv * sin
        mod = a * a + p * p
        cr = ((lr - 1.0) * a + li * p) / mod
        ci = (li * a - (lr - 1.0) * p) / mod
        one, zero = jnp.ones_like(a), jnp.zeros_like(a)
        pr, pi, mr, mi = one, zero, cr, ci
        sr, si, qr, qi = lr, li, nr, ni
        row = lax.broadcasted_iota(jnp.int32, a.shape, 0)
        for bit in range(3):
            on = lax.rem(row // (1 << bit), 2) == 1
            ar, ai = cmul(pr, pi, sr, si)
            pr, pi = jnp.where(on, ar, pr), jnp.where(on, ai, pi)
            ar, ai = cmul(mr, mi, qr, qi)
            mr, mi = jnp.where(on, ar, mr), jnp.where(on, ai, mi)
            sr, si = cmul(sr, si, sr, si)
            qr, qi = cmul(qr, qi, qr, qi)
        t2r[0:8, cut], t2i[0:8, cut], t1r[0:8, cut], t1i[0:8, cut] = pr, pi, mr, mi
        done = 8
        while done < rows:
            more = min(done, rows - done)
            for off in range(0, more, 8):
                src, dst = slice(off, off + 8), slice(done + off, done + off + 8)
                t2r[dst, cut], t2i[dst, cut] = cmul(t2r[src, cut], t2i[src, cut], sr, si)
                t1r[dst, cut], t1i[dst, cut] = cmul(t1r[src, cut], t1i[src, cut], qr, qi)
            sr, si = cmul(sr, si, sr, si)
            qr, qi = cmul(qr, qi, qr, qi)
            done += more
        lastr, lasti = t2r[rows - 1 : rows, cut], t2i[rows - 1 : rows, cut]
        wr, wi = cmul(lastr, lasti, lr[0:1], li[0:1])
        l_ref[blk : blk + 1, :] = wr
        l_ref[n_blk + blk : n_blk + blk + 1, :] = wi
        l_ref[2 * n_blk + blk : 2 * n_blk + blk + 1, :] = lr[0:1]
        l_ref[3 * n_blk + blk : 3 * n_blk + blk + 1, :] = li[0:1]

    pl.semaphore_wait(barrier, n_tp - 1 + around(1))

    sends = []
    for blk in range(n_blk):
        for k in range(1, n_tp):
            j = lax.rem(tp + n_tp - k, n_tp)
            copy = remote(
                nsend.at[j, blk], urecv.at[tp, blk], a_send.at[k, blk], a_recv.at[tp, blk], {"tp": j}
            )
            copy.start()
            sends.append(copy)
    if n_sp > 2:
        signal_sp(met.at[0], 1)
    for copy in loads[10:]:
        copy.start()
    urecv[tp] = nsend[tp]

    for copy in loads[4:10]:
        copy.wait()
    keep_c = (
        lax.broadcasted_iota(jnp.int32, (LANES, lanes), 0) // group
        == lax.broadcasted_iota(jnp.int32, (LANES, lanes), 1) // state
    )
    for blk in range(n_blk):
        for part, in_ref, out_ref in ((0, bre, cre), (1, bim, cim)):
            at = slice(part * lanes, (part + 1) * lanes)
            ch = slice(blk * LANES, (blk + 1) * LANES)
            b, c = in_ref[ch, :], out_ref[ch, :]
            wide = jnp.where(keep_c, jnp.concatenate([b] * per, axis=1), 0.0)
            bs[blk, :, at] = wide.astype(BF16)
            wide = jnp.where(keep_c, jnp.concatenate([c if part == 0 else -c] * per, axis=1), 0.0)
            cs[blk, :, at] = wide.astype(BF16)
    lower = (
        lax.broadcasted_iota(jnp.int32, (rows, rows), 0)
        >= lax.broadcasted_iota(jnp.int32, (rows, rows), 1)
    ).astype(BF16)

    d = 1
    hops = []
    while d < n_sp - 1:
        hops.append(d)
        d *= 2
    for r, d in enumerate(hops):
        if r > 0:
            signal_sp(met.at[r], d)
        if r < len(hops) - 1:
            pl.semaphore_wait(met.at[r], around(d))

    def end_copy(j, blk):
        return remote(
            e_send.at[blk], e_all.at[sp, blk], e_ssem.at[j, blk], e_rsem.at[sp, blk], {"sp": j}
        )

    for blk in range(n_blk):
        cut = slice(blk * lanes, (blk + 1) * lanes)
        ch = slice(blk * LANES, (blk + 1) * LANES)
        for k in range(1, n_tp):
            j = lax.rem(tp + k, n_tp)
            remote(
                nsend.at[j, blk], urecv.at[j, blk], a_send.at[k, blk], a_recv.at[j, blk], {"tp": j}
            ).wait_recv()
        for j in range(n_tp):
            uf[j * mine : (j + 1) * mine, ch] = urecv[j, blk].astype(F32)
        u = uf[:, ch].astype(BF16)
        d = jnp.dot(u, bs[blk], preferred_element_type=F32)
        wr, wi = cmul(d[:, :lanes], d[:, lanes:], t1r[:, cut], t1i[:, cut])
        wbuf[blk, :, :lanes] = wr.astype(BF16)
        wbuf[blk, :, lanes:] = wi.astype(BF16)
        er, ei = cmul(
            jnp.sum(wr, axis=0, keepdims=True), jnp.sum(wi, axis=0, keepdims=True),
            t2r[rows - 1 : rows, cut], t2i[rows - 1 : rows, cut],
        )
        e_send[blk] = jnp.concatenate([er, ei], axis=0).astype(BF16)

        if blk == 0 and hops:
            pl.semaphore_wait(met.at[len(hops) - 1], around(hops[-1]))

        def send_end(k, c, blk=blk):
            end_copy(n_sp - 1 - k, blk).start()
            return c

        lax.fori_loop(0, n_sp - 1 - sp, send_end, 0)

    for blk in range(n_blk):
        cut = slice(blk * lanes, (blk + 1) * lanes)
        s = jnp.dot(lower, wbuf[blk], preferred_element_type=F32)
        xr, xi = cmul(s[:, :lanes], s[:, lanes:], t2r[:, cut], t2i[:, cut])
        wbuf[blk, :, :lanes] = xr.astype(BF16)
        wbuf[blk, :, lanes:] = xi.astype(BF16)
        y = lax.dot_general(wbuf[blk], cs[blk], NT, preferred_element_type=F32)
        ch = slice(blk * LANES, (blk + 1) * LANES)
        ylocal[:, ch] = y + skip[:, ch] * uf[:, ch]

    for blk in range(n_blk):
        cut = slice(blk * lanes, (blk + 1) * lanes)
        ch = slice(blk * LANES, (blk + 1) * LANES)
        lr, li = l_ref[blk : blk + 1, :], l_ref[n_blk + blk : n_blk + blk + 1, :]

        def join(j, held, blk=blk, lr=lr, li=li):
            remote(
                e_send.at[blk], e_all.at[j, blk], e_ssem.at[j, blk], e_rsem.at[j, blk], {"sp": j}
            ).wait_recv()
            e = e_all[j, blk].astype(F32)
            hr, hi = cmul(*held, lr, li)
            return hr + e[0:1], hi + e[1:2]

        nil = jnp.zeros((1, lanes), F32)
        hr, hi = lax.fori_loop(0, sp, join, (nil, nil))
        hr, hi = cmul(
            hr, hi, l_ref[2 * n_blk + blk : 2 * n_blk + blk + 1, :], l_ref[3 * n_blk + blk : 3 * n_blk + blk + 1, :]
        )
        xr, xi = cmul(hr, hi, t2r[:, cut], t2i[:, cut])
        wbuf[blk, :, :lanes] = xr.astype(BF16)
        wbuf[blk, :, lanes:] = xi.astype(BF16)
        y = lax.dot_general(wbuf[blk], cs[blk], NT, preferred_element_type=F32)
        zbuf[tp, blk] = jax.nn.gelu(y + ylocal[:, ch]).astype(BF16)
        for k in range(1, n_chip):
            j = lax.rem(tp + 2 * k, n_tp)
            copy = remote(
                zbuf.at[tp, blk], zbuf.at[tp, blk], z_send.at[k, blk], z_recv.at[tp, blk], {"tp": j}
            )
            copy.start()
            sends.append(copy)
        copy = remote(
            zbuf.at[tp, blk], zbuf.at[tp, blk], z_send.at[0, blk], z_recv.at[tp, blk], {"tp": partner}
        )
        copy.start()
        sends.append(copy)

    for copy in loads[10:]:
        copy.wait()

    def arrived(j, blk):
        remote(
            zbuf.at[j, blk], zbuf.at[j, blk], z_send.at[0, blk], z_recv.at[j, blk], {"tp": partner}
        ).wait_recv()

    def project(j, blk, first=False):
        at = pl.ds(pl.multiple_of(j * width + blk * LANES, LANES), LANES)
        z = zbuf[j, blk]
        v = jnp.dot(z, wv[at, :], preferred_element_type=F32)
        g = jnp.dot(z, wg[at, :], preferred_element_type=F32)
        if first:
            acc_v[...], acc_g[...] = v, g
        else:
            acc_v[...] += v
            acc_g[...] += g

    for blk in range(n_blk):
        project(tp, blk, blk == 0)
    for blk in range(n_blk):
        arrived(partner, blk)
        project(partner, blk)
    late = []
    for blk in range(n_blk):
        for k in range(1, n_chip):
            j = lax.rem(tp + n_tp - 2 * k, n_tp)
            arrived(j, blk)
            copy = remote(
                zbuf.at[j, blk], zbuf.at[j, blk], f_send.at[k, blk], z_recv.at[j, blk], {"tp": partner}
            )
            copy.start()
            sends.append(copy)
            project(j, blk)
            late.append((lax.rem(partner + n_tp - 2 * k, n_tp), blk))
            if len(late) > 1:
                item = late.pop(0)
                arrived(*item)
                project(*item)
    for item in late:
        arrived(*item)
        project(*item)

    gated = acc_v[...] * jax.nn.sigmoid(acc_g[...])
    acc_v[...] = gated
    square = gated * gated
    part = square[:, :LANES]
    for blk in range(1, n_blk):
        part = part + square[:, blk * LANES : (blk + 1) * LANES]
    total = exact(jnp.ones((8, LANES), BF16), part)
    sq_all[tp] = total[0:1]
    for k in range(1, n_tp):
        j = lax.rem(tp + n_tp - k, n_tp)
        copy = remote(sq_all.at[tp], sq_all.at[tp], q_send.at[k], q_recv.at[tp], {"tp": j})
        copy.start()
        sends.append(copy)
    total = total[0:1]
    for k in range(1, n_tp):
        j = lax.rem(tp + k, n_tp)
        remote(sq_all.at[j], sq_all.at[j], q_send.at[k], q_recv.at[j], {"tp": j}).wait_recv()
        total = total + sq_all[j]
    scale = lax.rsqrt(total / d_model + NORM_EPS)
    eye = (
        lax.broadcasted_iota(jnp.int32, (rows, rows), 0)
        == lax.broadcasted_iota(jnp.int32, (rows, rows), 1)
    ).astype(BF16)
    column = exact(eye, jnp.broadcast_to(scale, (LANES, rows)))
    for blk in range(n_blk):
        ch = slice(blk * LANES, (blk + 1) * LANES)
        out[:, ch] = (acc_v[:, ch] * column * nout[:, ch]).astype(BF16)

    for copy in sends:
        copy.wait_send()

    def sent(j, c):
        for blk in range(n_blk):
            end_copy(j, blk).wait_send()
        return c

    lax.fori_loop(sp + 1, n_sp, sent, 0)


def solution(mesh):
    n_sp, n_tp = mesh.shape["sp"], mesh.shape["tp"]

    def on_device(
        tokens, norm_in, decay_log, phase, b_real, b_imag, c_real, c_imag, skip_gain, w_value, w_gate, norm_out
    ):
        mine, d_model = tokens.shape
        rows = mine * n_tp
        groups, state, group = b_real.shape
        width = groups * group
        n_blk = width // LANES
        lanes = LANES // group * state
        entries = groups * state
        vmem = pl.BlockSpec(memory_space=pltpu.VMEM)
        hbm = pl.BlockSpec(memory_space=pl.ANY)
        dma = pltpu.SemaphoreType.DMA
        return pl.pallas_call(
            functools.partial(layer, n_sp, n_tp, state, group),
            out_shape=pltpu.VMEM((rows, width), BF16),
            in_specs=[hbm] * 12,
            out_specs=vmem,
            scratch_shapes=[
                pltpu.VMEM((n_tp, n_blk, mine, LANES), BF16),
                pltpu.VMEM((n_tp, n_blk, mine, LANES), BF16),
                pltpu.VMEM((rows, width), F32),
                pltpu.VMEM((8, entries), F32),
                pltpu.VMEM((8, entries), F32),
                pltpu.VMEM((rows, entries), F32),
                pltpu.VMEM((rows, entries), F32),
                pltpu.VMEM((rows, entries), F32),
                pltpu.VMEM((rows, entries), F32),
                pltpu.VMEM((n_blk, LANES, 2 * lanes), BF16),
                pltpu.VMEM((n_blk, LANES, 2 * lanes), BF16),
                pltpu.VMEM((n_blk, rows, 2 * lanes), BF16),
                pltpu.VMEM((rows, width), F32),
                pltpu.VMEM((n_blk, 2, lanes), BF16),
                pltpu.VMEM((n_sp, n_blk, 2, lanes), BF16),
                pltpu.VMEM((4 * n_blk, lanes), F32),
                pltpu.VMEM((n_tp, n_blk, rows, LANES), BF16),
                pltpu.VMEM(w_value.shape, BF16),
                pltpu.VMEM(w_gate.shape, BF16),
                pltpu.VMEM((rows, width), F32),
                pltpu.VMEM((rows, width), F32),
                pltpu.VMEM((n_tp, 1, rows), F32),
                pltpu.VMEM((width, state), F32),
                pltpu.VMEM((width, state), F32),
                pltpu.VMEM((width, state), F32),
                pltpu.VMEM((width, state), F32),
                pltpu.VMEM((mine, d_model), BF16),
                pltpu.VMEM((1, d_model), F32),
                pltpu.VMEM((groups, state), F32),
                pltpu.VMEM((groups, state), F32),
                pltpu.VMEM((1, width), F32),
                pltpu.VMEM((1, width), F32),
                dma((12,)),
                dma((n_tp, n_blk)),
                dma((n_tp, n_blk)),
                dma((n_sp, n_blk)),
                dma((n_sp, n_blk)),
                dma((n_tp // 2, n_blk)),
                dma((n_tp, n_blk)),
                dma((n_tp // 2, n_blk)),
                dma((n_tp,)),
                dma((n_tp,)),
                pltpu.SemaphoreType.REGULAR((max(n_sp.bit_length(), 1),)),
            ],
            compiler_params=pltpu.CompilerParams(collective_id=0, has_side_effects=True),
        )(
            tokens,
            norm_in.reshape(1, -1),
            decay_log,
            phase,
            b_real.transpose(0, 2, 1).reshape(width, state),
            b_imag.transpose(0, 2, 1).reshape(width, state),
            c_real.reshape(width, state),
            c_imag.reshape(width, state),
            skip_gain.reshape(1, -1),
            w_value,
            w_gate,
            norm_out.reshape(1, -1),
        )

    placed = (
        P(("sp", "tp"), None),
        P(),
        P("tp", None),
        P("tp", None),
        P("tp", None, None),
        P("tp", None, None),
        P("tp", None, None),
        P("tp", None, None),
        P("tp"),
        P(None, "tp"),
        P(None, "tp"),
        P("tp"),
    )
    return jax.shard_map(
        on_device, mesh=mesh, in_specs=placed, out_specs=P("sp", "tp"), check_vma=False
    )
```

profile of v0, /device:TPU:0, one launch (start us, length us, event | category | flops | bytes accessed | tf_op | source)
XLA Modules:
  0.0 24.7 jit_solution(11874857493412559247)
XLA Ops:
  0.0 24.0 %shard_map.118 = bf16[192,512]{1,0:T(8,128)(2,1)S(1)} custom-call(bf16[48,2048]{1,0:T(8,128)(2,1)} %tok_h.1, f32[1,2048]{1,0:T(1,128)} %bitcast.15, f32[32,64]{1,0:T(8,128)} %dlog_h.1, f32[32,64]{1,0:T(8,128)} %phase_h.1, f32[512,64]{1,0:T(8,128)} %bitcast.11, f32[512,64]{1,0:T(8,128)} %bitcast.12, f32[512,64]{1,0:T(8,128)} %bitcast.13, f32[512,64]{1,0:T(8,128)} %bitcast.14, ...), custom_call_target="tpu_custom_call" | custom-call | tf_op jit(solution)/shard_map/pallas_call | solution.py:383
  24.0 0.7 %copy.14 = bf16[192,512]{1,0:T(8,128)(2,1)} copy(bf16[192,512]{1,0:T(8,128)(2,1)S(1)} %shard_map.118) | data formatting | bytes 393216
where the time goes:
time: 24.8 us; the launch traced here: 24.7 us
  Pallas kernels  24 us (97%)
  local copies, waits for them, and re-layouts  0.68 us (3%)
    pallas_call x1, Pallas kernels, on_device(): pl.pallas_call(functools.partial(layer, n_sp, n_tp, state, group), out_sh...  24 us
    unnamed x1, local copies, waits for them, and re-layouts  0.68 us

commit v1 on v0

v1 whole, which is shorter than its diff:
```python
import functools

import jax
import jax.numpy as jnp
from jax import lax
from jax.experimental import pallas as pl
from jax.experimental.pallas import tpu as pltpu
from jax.sharding import PartitionSpec as P

NORM_EPS = 1e-06
LANES = 128
F32 = jnp.float32
BF16 = jnp.bfloat16


def cmul(ar, ai, br, bi):
    return ar * br - ai * bi, ar * bi + ai * br


def cpow(r, i, n):
    outr, outi = None, None
    while n:
        if n % 2:
            outr, outi = (r, i) if outr is None else cmul(outr, outi, r, i)
        n //= 2
        if n:
            r, i = cmul(r, i, r, i)
    return outr, outi


def remote(src, dst, send, recv, target):
    return pltpu.make_async_remote_copy(
        src_ref=src,
        dst_ref=dst,
        send_sem=send,
        recv_sem=recv,
        device_id=target,
        device_id_type=pl.DeviceIdType.MESH,
    )


def layer(
    n_sp, n_tp, state, group,
    tok_h, nin_h, dlog_h, phase_h, bre_h, bim_h, cre_h, cim_h, skip_h, wv_h, wg_h, nout_h,
    out,
    nsend, urecv, rows_a, rows_p, t1r, t1i, t2r, t2i, bs, cs, wbuf, xbuf, wsum, ylocal,
    e_send, e_all, l_ref, zbuf, wv, wg, acc_v, acc_g, sq_all,
    bre, bim, cre, cim, tok, nin, dlog, phase, skip, nout,
    load_sem, a_send, a_recv, e_ssem, e_rsem, z_send, z_recv, f_send, q_send, q_recv, met,
):
    sp, tp = lax.axis_index("sp"), lax.axis_index("tp")
    mine, d_model = tok.shape
    rows, width = acc_v.shape
    n_blk = width // LANES
    per = LANES // group
    lanes = per * state
    core = lax.rem(tp, 2)
    chip = tp // 2
    partner = tp + 1 - 2 * core
    n_chip = n_tp // 2
    span = 2 * mine
    near = max(n_sp // 2, 1)

    loads = [
        pltpu.make_async_copy(src, dst, load_sem.at[i])
        for i, (src, dst) in enumerate(
            (
                (tok_h, tok), (nin_h, nin), (dlog_h, dlog), (phase_h, phase),
                (bre_h, bre), (bim_h, bim), (cre_h, cre), (cim_h, cim),
                (skip_h, skip), (nout_h, nout), (wv_h, wv), (wg_h, wg),
            )
        )
    ]
    for copy in loads[:4]:
        copy.start()

    barrier = pltpu.get_barrier_semaphore()
    for k in range(1, n_tp):
        pl.semaphore_signal(
            barrier, inc=1, device_id={"tp": lax.rem(tp + k, n_tp)},
            device_id_type=pl.DeviceIdType.MESH,
        )

    def greet(j, c):
        pl.semaphore_signal(barrier, inc=1, device_id={"sp": j}, device_id_type=pl.DeviceIdType.MESH)
        return c

    lax.fori_loop(sp + 1, n_sp, greet, 0)
    for copy in loads[4:10]:
        copy.start()
    for copy in loads[:2]:
        copy.wait()

    xf = tok[...].astype(F32)
    scale = lax.rsqrt(jnp.sum(xf * xf, axis=1, keepdims=True) / d_model + NORM_EPS)
    normed = (xf * scale * nin[...]).astype(BF16)
    for j in range(n_tp):
        for blk in range(n_blk):
            at = j * width + blk * LANES
            nsend[j, blk] = normed[:, at : at + LANES]

    pl.semaphore_wait(barrier, n_tp - 1 + sp)

    sends = []
    far_peers = []
    for k in range(1, n_chip):
        other = lax.rem(chip + n_chip - k, n_chip)
        far_peers += [2 * other + core, 2 * other + 1 - core]

    def scatter(i, j, blk):
        copy = remote(
            nsend.at[j, blk], urecv.at[tp, blk], a_send.at[i, blk], a_recv.at[tp, blk], {"tp": j}
        )
        copy.start()
        sends.append(copy)

    for blk in range(n_blk):
        for i, j in enumerate(far_peers):
            scatter(i, j, blk)
        if blk == 0:
            for b in range(n_blk):
                scatter(n_tp - 2, partner, b)

    def ready(j, c):
        pl.semaphore_signal(met.at[sp], inc=1, device_id={"sp": j}, device_id_type=pl.DeviceIdType.MESH)
        return c

    lax.fori_loop(0, sp, ready, 0)
    for copy in loads[10:]:
        copy.start()
    urecv[tp] = nsend[tp]

    for copy in loads[2:4]:
        copy.wait()
    side = LANES // state
    for i in range(width // group // side):
        cut = slice(i * LANES, (i + 1) * LANES)
        for src, dst in ((dlog, rows_a), (phase, rows_p)):
            row = jnp.concatenate([src[i * side + k : i * side + k + 1, :] for k in range(side)], axis=1)
            dst[:, cut] = jnp.broadcast_to(row, (8, LANES))

    for blk in range(n_blk):
        cut = slice(blk * lanes, (blk + 1) * lanes)
        a, p = rows_a[:, cut], rows_p[:, cut]
        mag, cos, sin = jnp.exp(a), jnp.cos(p), jnp.sin(p)
        lr, li = mag * cos, mag * sin
        inv = jnp.exp(-a)
        nr, ni = inv * cos, -inv * sin
        mod = a * a + p * p
        cr = ((lr - 1.0) * a + li * p) / mod
        ci = (li * a - (lr - 1.0) * p) / mod
        one, zero = jnp.ones_like(a), jnp.zeros_like(a)
        pr, pi, mr, mi = one, zero, cr, ci
        sr, si, qr, qi = lr, li, nr, ni
        row = lax.broadcasted_iota(jnp.int32, a.shape, 0)
        for bit in range(3):
            on = lax.rem(row // (1 << bit), 2) == 1
            ar, ai = cmul(pr, pi, sr, si)
            pr, pi = jnp.where(on, ar, pr), jnp.where(on, ai, pi)
            ar, ai = cmul(mr, mi, qr, qi)
            mr, mi = jnp.where(on, ar, mr), jnp.where(on, ai, mi)
            sr, si = cmul(sr, si, sr, si)
            qr, qi = cmul(qr, qi, qr, qi)
        t2r[0:8, cut], t2i[0:8, cut], t1r[0:8, cut], t1i[0:8, cut] = pr, pi, mr, mi
        done = 8
        while done < span:
            more = min(done, span - done)
            for off in range(0, more, 8):
                src, dst = slice(off, off + 8), slice(done + off, done + off + 8)
                t2r[dst, cut], t2i[dst, cut] = cmul(t2r[src, cut], t2i[src, cut], sr, si)
                t1r[dst, cut], t1i[dst, cut] = cmul(t1r[src, cut], t1i[src, cut], qr, qi)
            sr, si = cmul(sr, si, sr, si)
            qr, qi = cmul(qr, qi, qr, qi)
            done += more
        endr, endi = t2r[span - 1 : span, cut], t2i[span - 1 : span, cut]
        wholer, wholei = cmul(endr, endi, lr[0:1], li[0:1])
        allr, alli = cpow(wholer, wholei, n_chip)
        for k, value in enumerate((allr, alli, lr[0:1], li[0:1], wholer, wholei, endr, endi)):
            l_ref[blk, k : k + 1, :] = value

    for copy in loads[4:10]:
        copy.wait()
    keep_b = (
        lax.broadcasted_iota(jnp.int32, (LANES, lanes), 0) // group
        == lax.broadcasted_iota(jnp.int32, (LANES, lanes), 1) // state
    )
    of_col = lax.broadcasted_iota(jnp.int32, (state, LANES), 1) // group
    a, p = dlog[...], phase[...]
    mag = jnp.exp(a)
    stepr, stepi = cpow(mag * jnp.cos(p), mag * jnp.sin(p), span)
    for blk in range(n_blk):
        ch = slice(blk * LANES, (blk + 1) * LANES)
        for part, in_ref in ((0, bre), (1, bim)):
            b = in_ref[ch, :]
            b = jnp.concatenate([b] * side, axis=1)
            wide = jnp.where(keep_b, jnp.concatenate([b] * (lanes // LANES), axis=1), 0.0)
            bs[blk, :, part * lanes : (part + 1) * lanes] = wide.astype(BF16)
        c_r, c_i = cre[ch, :], cim[ch, :]
        if n_chip > 1:
            spread = [
                jnp.concatenate(
                    [jnp.broadcast_to(s[g : g + 1], (group, state)) for g in range(blk * per, (blk + 1) * per)],
                    axis=0,
                )
                for s in (stepr, stepi)
            ]
        for c in range(n_chip):
            if c:
                c_r, c_i = cmul(c_r, c_i, *spread)
            turned = jnp.concatenate([c_r, -c_i], axis=1).T
            for part in range(2):
                piece = turned[part * state : (part + 1) * state]
                for g in range(per):
                    at = part * lanes + g * state
                    cs[blk, at : at + state, c * LANES : (c + 1) * LANES] = jnp.where(
                        of_col == g, piece, 0.0
                    ).astype(BF16)
    lower = (
        lax.broadcasted_iota(jnp.int32, (span, span), 0)
        >= lax.broadcasted_iota(jnp.int32, (span, span), 1)
    ).astype(BF16)

    def taken(j, blk):
        remote(
            nsend.at[j, blk], urecv.at[j, blk], a_send.at[0, blk], a_recv.at[j, blk], {"tp": partner}
        ).wait_recv()

    def source(c, blk):
        return jnp.concatenate([urecv[2 * c + s, blk].astype(F32) for s in range(2)], axis=0)

    def drive(c, blk):
        cut = slice(blk * lanes, (blk + 1) * lanes)
        d = jnp.dot(source(c, blk).astype(BF16), bs[blk], preferred_element_type=F32)
        wr, wi = cmul(d[:, :lanes], d[:, lanes:], t1r[:, cut], t1i[:, cut])
        wbuf[c, blk, :, :lanes] = wr.astype(BF16)
        wbuf[c, blk, :, lanes:] = wi.astype(BF16)
        wsum[c, blk, 0:1, :] = jnp.sum(wr, axis=0, keepdims=True)
        wsum[c, blk, 1:2, :] = jnp.sum(wi, axis=0, keepdims=True)

    def seeds(blk):
        turn = l_ref[blk, 4:5], l_ref[blk, 5:6]
        held = [None]
        for c in range(n_chip):
            r, i = wsum[c, blk, 0:1], wsum[c, blk, 1:2]
            if c:
                r, i = r + held[c][0], i + held[c][1]
            held.append(cmul(r, i, *turn) if c < n_chip - 1 else cmul(r, i, l_ref[blk, 6:7], l_ref[blk, 7:8]))
        return held

    def end_copy(j, blk):
        return remote(
            e_send.at[blk], e_all.at[sp, blk], e_ssem.at[j, blk], e_rsem.at[sp, blk], {"sp": j}
        )

    def local(blk):
        cut = slice(blk * lanes, (blk + 1) * lanes)
        ch = slice(blk * LANES, (blk + 1) * LANES)
        held = seeds(blk)
        for c in range(n_chip):
            s = jnp.dot(lower, wbuf[c, blk], preferred_element_type=F32)
            sr, si = s[:, :lanes], s[:, lanes:]
            if c:
                sr, si = sr + held[c][0], si + held[c][1]
            xr, xi = cmul(sr, si, t2r[:, cut], t2i[:, cut])
            at = slice(c * span, (c + 1) * span)
            xbuf[blk, at, :lanes] = xr.astype(BF16)
            xbuf[blk, at, lanes:] = xi.astype(BF16)
        y = jnp.dot(xbuf[blk], cs[blk, :, :LANES], preferred_element_type=F32)
        for c in range(n_chip):
            at = slice(c * span, (c + 1) * span)
            ylocal[blk, at] = y[at] + skip[:, ch] * source(c, blk)

    for blk in range(n_blk):
        taken(partner, blk)
    for blk in range(n_blk):
        drive(chip, blk)

    def send_ends(blk, first, last):
        def go(j, c):
            end_copy(j, blk).start()
            return c

        lax.fori_loop(first, last, go, 0)

    def meet(first, last):
        def go(j, c):
            pl.semaphore_wait(met.at[j], 1)
            return c

        lax.fori_loop(first, last, go, 0)

    close = jnp.minimum(sp + 1 + near, n_sp)
    for blk in range(n_blk):
        for k in range(1, n_chip):
            c = lax.rem(chip + k, n_chip)
            taken(2 * c, blk)
            taken(2 * c + 1, blk)
        for k in range(1, n_chip):
            drive(lax.rem(chip + k, n_chip), blk)
        er, ei = seeds(blk)[n_chip]
        e_send[blk] = jnp.concatenate([er, ei], axis=0).astype(BF16)
        if blk:
            local(blk - 1)
        if blk == 0:
            meet(sp + 1, close)
        send_ends(blk, sp + 1, close)
    local(n_blk - 1)

    def send_far():
        meet(close, n_sp)
        for blk in range(n_blk):
            send_ends(blk, close, n_sp)

    pl.when(sp > 0)(send_far)

    for blk in range(n_blk):
        cut = slice(blk * lanes, (blk + 1) * lanes)
        lr, li = l_ref[blk, 0:1], l_ref[blk, 1:2]

        def join(j, held, blk=blk, lr=lr, li=li):
            remote(
                e_send.at[blk], e_all.at[j, blk], e_ssem.at[j, blk], e_rsem.at[j, blk], {"sp": j}
            ).wait_recv()
            e = e_all[j, blk].astype(F32)
            hr, hi = cmul(*held, lr, li)
            return hr + e[0:1], hi + e[1:2]

        nil = jnp.zeros((1, lanes), F32)
        hr, hi = lax.fori_loop(0, sp, join, (nil, nil))
        hr, hi = cmul(hr, hi, l_ref[blk, 2:3], l_ref[blk, 3:4])
        xr, xi = cmul(hr, hi, t2r[:, cut], t2i[:, cut])
        x = jnp.concatenate([xr.astype(BF16), xi.astype(BF16)], axis=1)
        y = jnp.dot(x, cs[blk], preferred_element_type=F32)
        for c in range(n_chip):
            at = slice(c * span, (c + 1) * span)
            zbuf[tp, blk, at] = jax.nn.gelu(y[:, c * LANES : (c + 1) * LANES] + ylocal[blk, at]).astype(BF16)
        for k in range(1, n_chip):
            j = lax.rem(tp + 2 * k, n_tp)
            copy = remote(
                zbuf.at[tp, blk], zbuf.at[tp, blk], z_send.at[k, blk], z_recv.at[tp, blk], {"tp": j}
            )
            copy.start()
            sends.append(copy)
        copy = remote(
            zbuf.at[tp, blk], zbuf.at[tp, blk], z_send.at[0, blk], z_recv.at[tp, blk], {"tp": partner}
        )
        copy.start()
        sends.append(copy)
    pl.when(sp == 0)(send_far)

    for copy in loads[10:]:
        copy.wait()

    def arrived(j, blk):
        remote(
            zbuf.at[j, blk], zbuf.at[j, blk], z_send.at[0, blk], z_recv.at[j, blk], {"tp": partner}
        ).wait_recv()

    def project(items):
        at = [pl.ds(pl.multiple_of(j * width + blk * LANES, LANES), LANES) for j, blk in items]
        z = jnp.concatenate([zbuf[j, blk] for j, blk in items], axis=1)
        return [
            jnp.dot(z, jnp.concatenate([w[a, :] for a in at], axis=0), preferred_element_type=F32)
            for w in (wv, wg)
        ]

    v, g = project([(tp, blk) for blk in range(n_blk)])
    acc_v[...], acc_g[...] = v, g
    for blk in range(n_blk):
        arrived(partner, blk)
    v, g = project([(partner, blk) for blk in range(n_blk)])
    acc_v[...] += v
    acc_g[...] += g
    late = []
    ripe = []

    def flush():
        v, g = project(ripe)
        ripe.clear()
        acc_v[...] += v
        acc_g[...] += g

    for blk in range(n_blk):
        for k in range(1, n_chip):
            j = lax.rem(tp + n_tp - 2 * k, n_tp)
            arrived(j, blk)
            copy = remote(
                zbuf.at[j, blk], zbuf.at[j, blk], f_send.at[k, blk], z_recv.at[j, blk], {"tp": partner}
            )
            copy.start()
            sends.append(copy)
            ripe.append((j, blk))
            if len(ripe) == 2:
                flush()
            late.append((lax.rem(partner + n_tp - 2 * k, n_tp), blk))
            if len(late) > 1:
                item = late.pop(0)
                arrived(*item)
                ripe.append(item)
                if len(ripe) == 2:
                    flush()
    if ripe:
        flush()
    for item in late:
        arrived(*item)
    if late:
        v, g = project(late)
        v, g = acc_v[...] + v, acc_g[...] + g
    else:
        v, g = acc_v[...], acc_g[...]

    gated = v * (0.5 + 0.5 * jnp.tanh(0.5 * g))
    acc_v[...] = gated
    square = gated * gated
    part = square[:, :LANES]
    for blk in range(1, n_blk):
        part = part + square[:, blk * LANES : (blk + 1) * LANES]
    sums = jnp.sum(part, axis=1, keepdims=True)
    lane = lax.broadcasted_iota(jnp.int32, (8, LANES), 1)
    total = jnp.zeros((8, LANES), F32)
    for k in range(rows // 8):
        total = jnp.where(lane == k, sums[8 * k : 8 * k + 8], total)
    sq_all[tp] = total
    for k in range(1, n_tp):
        j = lax.rem(tp + n_tp - k, n_tp)
        copy = remote(sq_all.at[tp], sq_all.at[tp], q_send.at[k], q_recv.at[tp], {"tp": j})
        copy.start()
        sends.append(copy)
    for k in range(1, n_tp):
        j = lax.rem(tp + k, n_tp)
        remote(sq_all.at[j], sq_all.at[j], q_send.at[k], q_recv.at[j], {"tp": j}).wait_recv()
        total = total + sq_all[j]
    scale = lax.rsqrt(total / d_model + NORM_EPS)
    for k in range(0, rows // 8, 2):
        two = range(k, min(k + 2, rows // 8))
        column = jnp.concatenate([scale[:, i : i + 1] for i in two], axis=0)
        at = slice(8 * k, 8 * k + 8 * len(two))
        out[at, :] = (acc_v[at, :] * column * nout[...]).astype(BF16)

    for copy in sends:
        copy.wait_send()

    def sent(j, c):
        for blk in range(n_blk):
            end_copy(j, blk).wait_send()
        return c

    lax.fori_loop(sp + 1, n_sp, sent, 0)


def solution(mesh):
    n_sp, n_tp = mesh.shape["sp"], mesh.shape["tp"]

    def on_device(
        tokens, norm_in, decay_log, phase, b_real, b_imag, c_real, c_imag, skip_gain, w_value, w_gate, norm_out
    ):
        mine, d_model = tokens.shape
        rows = mine * n_tp
        groups, state, group = b_real.shape
        width = groups * group
        n_blk = width // LANES
        lanes = LANES // group * state
        entries = groups * state
        n_chip = n_tp // 2
        span = 2 * mine
        vmem = pl.BlockSpec(memory_space=pltpu.VMEM)
        hbm = pl.BlockSpec(memory_space=pl.ANY)
        dma = pltpu.SemaphoreType.DMA
        return pl.pallas_call(
            functools.partial(layer, n_sp, n_tp, state, group),
            out_shape=pltpu.VMEM((rows, width), BF16),
            in_specs=[hbm] * 12,
            out_specs=vmem,
            scratch_shapes=[
                pltpu.VMEM((n_tp, n_blk, mine, LANES), BF16),
                pltpu.VMEM((n_tp, n_blk, mine, LANES), BF16),
                pltpu.VMEM((8, entries), F32),
                pltpu.VMEM((8, entries), F32),
                pltpu.VMEM((span, entries), F32),
                pltpu.VMEM((span, entries), F32),
                pltpu.VMEM((span, entries), F32),
                pltpu.VMEM((span, entries), F32),
                pltpu.VMEM((n_blk, LANES, 2 * lanes), BF16),
                pltpu.VMEM((n_blk, 2 * lanes, n_chip * LANES), BF16),
                pltpu.VMEM((n_chip, n_blk, span, 2 * lanes), BF16),
                pltpu.VMEM((n_blk, rows, 2 * lanes), BF16),
                pltpu.VMEM((n_chip, n_blk, 2, lanes), F32),
                pltpu.VMEM((n_blk, rows, LANES), F32),
                pltpu.VMEM((n_blk, 2, lanes), BF16),
                pltpu.VMEM((n_sp, n_blk, 2, lanes), BF16),
                pltpu.VMEM((n_blk, 8, lanes), F32),
                pltpu.VMEM((n_tp, n_blk, rows, LANES), BF16),
                pltpu.VMEM(w_value.shape, BF16),
                pltpu.VMEM(w_gate.shape, BF16),
                pltpu.VMEM((rows, width), F32),
                pltpu.VMEM((rows, width), F32),
                pltpu.VMEM((n_tp, 8, LANES), F32),
                pltpu.VMEM((width, state), F32),
                pltpu.VMEM((width, state), F32),
                pltpu.VMEM((width, state), F32),
                pltpu.VMEM((width, state), F32),
                pltpu.VMEM((mine, d_model), BF16),
                pltpu.VMEM((1, d_model), F32),
                pltpu.VMEM((groups, state), F32),
                pltpu.VMEM((groups, state), F32),
                pltpu.VMEM((1, width), F32),
                pltpu.VMEM((1, width), F32),
                dma((12,)),
                dma((n_tp - 1, n_blk)),
                dma((n_tp, n_blk)),
                dma((n_sp, n_blk)),
                dma((n_sp, n_blk)),
                dma((n_chip, n_blk)),
                dma((n_tp, n_blk)),
                dma((n_chip, n_blk)),
                dma((n_tp,)),
                dma((n_tp,)),
                pltpu.SemaphoreType.REGULAR((n_sp,)),
            ],
            compiler_params=pltpu.CompilerParams(collective_id=0, has_side_effects=True),
        )(
            tokens,
            norm_in.reshape(1, -1),
            decay_log,
            phase,
            b_real.transpose(0, 2, 1).reshape(width, state),
            b_imag.transpose(0, 2, 1).reshape(width, state),
            c_real.reshape(width, state),
            c_imag.reshape(width, state),
            skip_gain.reshape(1, -1),
            w_value,
            w_gate,
            norm_out.reshape(1, -1),
        )

    placed = (
        P(("sp", "tp"), None),
        P(),
        P("tp", None),
        P("tp", None),
        P("tp", None, None),
        P("tp", None, None),
        P("tp", None, None),
        P("tp", None, None),
        P("tp"),
        P(None, "tp"),
        P(None, "tp"),
        P("tp"),
    )
    return jax.shard_map(
        on_device, mesh=mesh, in_specs=placed, out_specs=P("sp", "tp"), check_vma=False
    )
```

time: 24.8 us -> 22.5 us (0.907)
  the two profiles are of different devices: /device:TPU:0 before, /device:TPU:24 now
where the time goes in v1:
time: 22.5 us; the launch traced here: 22.4 us
  Pallas kernels  21.7 us (96%)
  local copies, waits for them, and re-layouts  0.68 us (3%)
    pallas_call x1, Pallas kernels, on_device(): pl.pallas_call(functools.partial(layer, n_sp, n_tp, state, group), out_sh...  21.7 us
    unnamed x1, local copies, waits for them, and re-layouts  0.68 us

profile of v1, /device:TPU:24, one launch (start us, length us, event | category | flops | bytes accessed | tf_op | source)
XLA Modules:
  0.0 22.4 jit_solution(5826214986351659657)
XLA Ops:
  0.0 21.7 %shard_map.118 = bf16[192,512]{1,0:T(8,128)(2,1)S(1)} custom-call(bf16[48,2048]{1,0:T(8,128)(2,1)} %tok_h.1, f32[1,2048]{1,0:T(1,128)} %bitcast.15, f32[32,64]{1,0:T(8,128)} %dlog_h.1, f32[32,64]{1,0:T(8,128)} %phase_h.1, f32[512,64]{1,0:T(8,128)} %bitcast.11, f32[512,64]{1,0:T(8,128)} %bitcast.12, f32[512,64]{1,0:T(8,128)} %bitcast.13, f32[512,64]{1,0:T(8,128)} %bitcast.14, ...), custom_call_target="tpu_custom_call" | custom-call | tf_op jit(solution)/shard_map/pallas_call | solution.py:469
  21.7 0.7 %copy.14 = bf16[192,512]{1,0:T(8,128)(2,1)} copy(bf16[192,512]{1,0:T(8,128)(2,1)S(1)} %shard_map.118) | data formatting | bytes 393216

commit v2 on v1

--- a/solution.py
+++ b/solution.py
@@ -46,7 +46,7 @@
     nsend, urecv, rows_a, rows_p, t1r, t1i, t2r, t2i, bs, cs, wbuf, xbuf, wsum, ylocal,
     e_send, e_all, l_ref, zbuf, wv, wg, acc_v, acc_g, sq_all,
     bre, bim, cre, cim, tok, nin, dlog, phase, skip, nout,
-    load_sem, a_send, a_recv, e_ssem, e_rsem, z_send, z_recv, f_send, q_send, q_recv, met,
+    load_sem, a_send, a_recv, e_ssem, e_rsem, z_send, z_recv, f_send, q_send, q_recv, met, met_tp,
 ):
     sp, tp = lax.axis_index("sp"), lax.axis_index("tp")
     mine, d_model = tok.shape
@@ -59,7 +59,8 @@
     partner = tp + 1 - 2 * core
     n_chip = n_tp // 2
     span = 2 * mine
-    near = max(n_sp // 2, 1)
+    pair = 2 if n_sp % 2 == 0 else 1
+    sp_b = lax.rem(sp, pair)
 
     loads = [
         pltpu.make_async_copy(src, dst, load_sem.at[i])
@@ -75,19 +76,32 @@
         copy.start()
 
     barrier = pltpu.get_barrier_semaphore()
-    for k in range(1, n_tp):
-        pl.semaphore_signal(
-            barrier, inc=1, device_id={"tp": lax.rem(tp + k, n_tp)},
-            device_id_type=pl.DeviceIdType.MESH,
-        )
-
-    def greet(j, c):
-        pl.semaphore_signal(barrier, inc=1, device_id={"sp": j}, device_id_type=pl.DeviceIdType.MESH)
-        return c
-
-    lax.fori_loop(sp + 1, n_sp, greet, 0)
+
+    def tell(sem, axis):
+        def go(j, c):
+            pl.semaphore_signal(sem, inc=1, device_id={axis: j}, device_id_type=pl.DeviceIdType.MESH)
+            return c
+
+        return go
+
+    def above(go):
+        for b in range(pair):
+            first = sp // pair + jnp.where(b > sp_b, 0, 1)
+            go_b = lambda a, c, b=b: go(a * pair + b, c)
+            lax.fori_loop(jnp.where(b >= sp_b, first, n_sp // pair), n_sp // pair, go_b, 0)
+
+    def below(go):
+        for b in range(pair):
+            last = sp // pair + jnp.where(b < sp_b, 1, 0)
+            lax.fori_loop(0, jnp.where(b <= sp_b, last, 0), lambda a, c, b=b: go(a * pair + b, c), 0)
+
+    lax.fori_loop(tp + 1, n_tp, tell(barrier, "tp"), 0)
+    above(tell(barrier, "sp"))
     for copy in loads[4:10]:
         copy.start()
+    pl.when(tp + sp > 0)(lambda: pl.semaphore_wait(barrier, tp + (sp // pair + 1) * (sp_b + 1) - 1))
+    below(tell(met.at[sp], "sp"))
+    lax.fori_loop(0, tp, tell(met_tp.at[tp], "tp"), 0)
     for copy in loads[:2]:
         copy.wait()
 
@@ -99,7 +113,14 @@
             at = j * width + blk * LANES
             nsend[j, blk] = normed[:, at : at + LANES]
 
-    pl.semaphore_wait(barrier, n_tp - 1 + sp)
+    def meet(sem):
+        def go(j, c):
+            pl.semaphore_wait(sem.at[j], 1)
+            return c
+
+        return go
+
+    lax.fori_loop(tp + 1, n_tp, meet(met_tp), 0)
 
     sends = []
     far_peers = []
@@ -121,11 +142,6 @@
             for b in range(n_blk):
                 scatter(n_tp - 2, partner, b)
 
-    def ready(j, c):
-        pl.semaphore_signal(met.at[sp], inc=1, device_id={"sp": j}, device_id_type=pl.DeviceIdType.MESH)
-        return c
-
-    lax.fori_loop(0, sp, ready, 0)
     for copy in loads[10:]:
         copy.start()
     urecv[tp] = nsend[tp]
@@ -232,16 +248,16 @@
         cut = slice(blk * lanes, (blk + 1) * lanes)
         d = jnp.dot(source(c, blk).astype(BF16), bs[blk], preferred_element_type=F32)
         wr, wi = cmul(d[:, :lanes], d[:, lanes:], t1r[:, cut], t1i[:, cut])
-        wbuf[c, blk, :, :lanes] = wr.astype(BF16)
-        wbuf[c, blk, :, lanes:] = wi.astype(BF16)
-        wsum[c, blk, 0:1, :] = jnp.sum(wr, axis=0, keepdims=True)
-        wsum[c, blk, 1:2, :] = jnp.sum(wi, axis=0, keepdims=True)
+        wbuf[blk][c, :, :lanes] = wr.astype(BF16)
+        wbuf[blk][c, :, lanes:] = wi.astype(BF16)
+        wsum[blk][c, 0:1, :] = jnp.sum(wr, axis=0, keepdims=True)
+        wsum[blk][c, 1:2, :] = jnp.sum(wi, axis=0, keepdims=True)
 
     def seeds(blk):
         turn = l_ref[blk, 4:5], l_ref[blk, 5:6]
         held = [None]
         for c in range(n_chip):
-            r, i = wsum[c, blk, 0:1], wsum[c, blk, 1:2]
+            r, i = wsum[blk][c, 0:1], wsum[blk][c, 1:2]
             if c:
                 r, i = r + held[c][0], i + held[c][1]
             held.append(cmul(r, i, *turn) if c < n_chip - 1 else cmul(r, i, l_ref[blk, 6:7], l_ref[blk, 7:8]))
@@ -252,72 +268,97 @@
             e_send.at[blk], e_all.at[sp, blk], e_ssem.at[j, blk], e_rsem.at[sp, blk], {"sp": j}
         )
 
-    def local(blk):
+    def scan(blk):
         cut = slice(blk * lanes, (blk + 1) * lanes)
-        ch = slice(blk * LANES, (blk + 1) * LANES)
         held = seeds(blk)
         for c in range(n_chip):
-            s = jnp.dot(lower, wbuf[c, blk], preferred_element_type=F32)
+            s = jnp.dot(lower, wbuf[blk][c], preferred_element_type=F32)
             sr, si = s[:, :lanes], s[:, lanes:]
             if c:
                 sr, si = sr + held[c][0], si + held[c][1]
             xr, xi = cmul(sr, si, t2r[:, cut], t2i[:, cut])
             at = slice(c * span, (c + 1) * span)
-            xbuf[blk, at, :lanes] = xr.astype(BF16)
-            xbuf[blk, at, lanes:] = xi.astype(BF16)
-        y = jnp.dot(xbuf[blk], cs[blk, :, :LANES], preferred_element_type=F32)
+            xbuf[blk][at, :lanes] = xr.astype(BF16)
+            xbuf[blk][at, lanes:] = xi.astype(BF16)
+
+    def readout(blk):
+        ch = slice(blk * LANES, (blk + 1) * LANES)
+        y = jnp.dot(xbuf[blk][...], cs[blk, :, :LANES], preferred_element_type=F32)
         for c in range(n_chip):
             at = slice(c * span, (c + 1) * span)
-            ylocal[blk, at] = y[at] + skip[:, ch] * source(c, blk)
+            ylocal[blk][at] = y[at] + skip[:, ch] * source(c, blk)
 
     for blk in range(n_blk):
         taken(partner, blk)
     for blk in range(n_blk):
         drive(chip, blk)
 
-    def send_ends(blk, first, last):
+    def send_ends(blks, first, last):
         def go(j, c):
-            end_copy(j, blk).start()
+            for blk in blks:
+                end_copy(j, blk).start()
             return c
 
         lax.fori_loop(first, last, go, 0)
 
-    def meet(first, last):
-        def go(j, c):
-            pl.semaphore_wait(met.at[j], 1)
-            return c
-
-        lax.fori_loop(first, last, go, 0)
-
-    close = jnp.minimum(sp + 1 + near, n_sp)
-    for blk in range(n_blk):
-        for k in range(1, n_chip):
-            c = lax.rem(chip + k, n_chip)
-            taken(2 * c, blk)
-            taken(2 * c + 1, blk)
-        for k in range(1, n_chip):
-            drive(lax.rem(chip + k, n_chip), blk)
-        er, ei = seeds(blk)[n_chip]
-        e_send[blk] = jnp.concatenate([er, ei], axis=0).astype(BF16)
-        if blk:
-            local(blk - 1)
-        if blk == 0:
-            meet(sp + 1, close)
-        send_ends(blk, sp + 1, close)
-    local(n_blk - 1)
-
-    def send_far():
-        meet(close, n_sp)
-        for blk in range(n_blk):
-            send_ends(blk, close, n_sp)
-
-    pl.when(sp > 0)(send_far)
-
-    for blk in range(n_blk):
+    def finish(blk, y):
+        for c in range(n_chip):
+            at = slice(c * span, (c + 1) * span)
+            v = ylocal[blk][at]
+            if y is not None:
+                v = v + y[:, c * LANES : (c + 1) * LANES]
+            zbuf[tp, blk, at] = jax.nn.gelu(v).astype(BF16)
+        for copy in z_copies(blk):
+            copy.start()
+
+    def z_copies(blk):
+        return [
+            remote(
+                zbuf.at[tp, blk], zbuf.at[tp, blk], z_send.at[k, blk], z_recv.at[tp, blk],
+                {"tp": lax.rem(tp + 2 * k, n_tp) if k else partner},
+            )
+            for k in list(range(1, n_chip)) + [0]
+        ]
+
+    def reach(j, c):
+        odd = lax.rem(j, pair)
+
+        @pl.when((sp_b == 0) | (odd == 0))
+        def _():
+            pl.semaphore_wait(met.at[jnp.where(sp_b == 0, j, j - odd + pair - 1)], 1)
+
+        return c
+
+    old = sp + 1
+    for blk in range(n_blk + 2):
+        if blk < n_blk:
+            for k in range(1, n_chip):
+                c = lax.rem(chip + k, n_chip)
+                taken(2 * c, blk)
+                taken(2 * c + 1, blk)
+            for k in range(1, n_chip):
+                drive(lax.rem(chip + k, n_chip), blk)
+        if 1 <= blk <= n_blk:
+            scan(blk - 1)
+        if 2 <= blk:
+            readout(blk - 2)
+        if blk < n_blk:
+            er, ei = seeds(blk)[n_chip]
+            e_send[blk] = jnp.concatenate([er, ei], axis=0).astype(BF16)
+            new = jnp.minimum(sp + 1 + n_sp // 2, n_sp) if blk == 0 else n_sp
+            lax.fori_loop(old, new, reach, 0)
+            if blk:
+                send_ends([blk], sp + 1, old)
+            send_ends(range(blk + 1), old, new)
+            old = new
+        if 2 <= blk:
+            pl.when(sp == 0)(functools.partial(finish, blk - 2, None))
+
+    def after(blk):
         cut = slice(blk * lanes, (blk + 1) * lanes)
         lr, li = l_ref[blk, 0:1], l_ref[blk, 1:2]
 
-        def join(j, held, blk=blk, lr=lr, li=li):
+        def join(j, held):
             remote(
                 e_send.at[blk], e_all.at[j, blk], e_ssem.at[j, blk], e_rsem.at[j, blk], {"sp": j}
             ).wait_recv()
@@ -330,23 +371,13 @@
         hr, hi = cmul(hr, hi, l_ref[blk, 2:3], l_ref[blk, 3:4])
         xr, xi = cmul(hr, hi, t2r[:, cut], t2i[:, cut])
         x = jnp.concatenate([xr.astype(BF16), xi.astype(BF16)], axis=1)
-        y = jnp.dot(x, cs[blk], preferred_element_type=F32)
-        for c in range(n_chip):
-            at = slice(c * span, (c + 1) * span)
-            zbuf[tp, blk, at] = jax.nn.gelu(y[:, c * LANES : (c + 1) * LANES] + ylocal[blk, at]).astype(BF16)
-        for k in range(1, n_chip):
-            j = lax.rem(tp + 2 * k, n_tp)
-            copy = remote(
-                zbuf.at[tp, blk], zbuf.at[tp, blk], z_send.at[k, blk], z_recv.at[tp, blk], {"tp": j}
-            )
-            copy.start()
-            sends.append(copy)
-        copy = remote(
-            zbuf.at[tp, blk], zbuf.at[tp, blk], z_send.at[0, blk], z_recv.at[tp, blk], {"tp": partner}
-        )
-        copy.start()
-        sends.append(copy)
-    pl.when(sp == 0)(send_far)
+        finish(blk, jnp.dot(x, cs[blk], preferred_element_type=F32))
+
+
+    @pl.when(sp > 0)
+    def _():
+        for blk in range(n_blk):
+            after(blk)
 
     for copy in loads[10:]:
         copy.wait()
@@ -421,11 +452,23 @@
     for k in range(rows // 8):
         total = jnp.where(lane == k, sums[8 * k : 8 * k + 8], total)
     sq_all[tp] = total
+    sums_out = []
     for k in range(1, n_tp):
         j = lax.rem(tp + n_tp - k, n_tp)
         copy = remote(sq_all.at[tp], sq_all.at[tp], q_send.at[k], q_recv.at[tp], {"tp": j})
         copy.start()
-        sends.append(copy)
+        sums_out.append(copy)
+    for blk in range(n_blk):
+        sends += z_copies(blk)
+    for copy in sends:
+        copy.wait_send()
+
+    def sent(j, c):
+        for blk in range(n_blk):
+            end_copy(j, blk).wait_send()
+        return c
+
+    lax.fori_loop(sp + 1, n_sp, sent, 0)
     for k in range(1, n_tp):
         j = lax.rem(tp + k, n_tp)
         remote(sq_all.at[j], sq_all.at[j], q_send.at[k], q_recv.at[j], {"tp": j}).wait_recv()
@@ -437,15 +480,8 @@
         at = slice(8 * k, 8 * k + 8 * len(two))
         out[at, :] = (acc_v[at, :] * column * nout[...]).astype(BF16)
 
-    for copy in sends:
+    for copy in sums_out:
         copy.wait_send()
-
-    def sent(j, c):
-        for blk in range(n_blk):
-            end_copy(j, blk).wait_send()
-        return c
-
-    lax.fori_loop(sp + 1, n_sp, sent, 0)
 
 
 def solution(mesh):
@@ -482,10 +518,10 @@
                 pltpu.VMEM((span, entries), F32),
                 pltpu.VMEM((n_blk, LANES, 2 * lanes), BF16),
                 pltpu.VMEM((n_blk, 2 * lanes, n_chip * LANES), BF16),
-                pltpu.VMEM((n_chip, n_blk, span, 2 * lanes), BF16),
-                pltpu.VMEM((n_blk, rows, 2 * lanes), BF16),
-                pltpu.VMEM((n_chip, n_blk, 2, lanes), F32),
-                pltpu.VMEM((n_blk, rows, LANES), F32),
+                [pltpu.VMEM((n_chip, span, 2 * lanes), BF16)] * n_blk,
+                [pltpu.VMEM((rows, 2 * lanes), BF16)] * n_blk,
+                [pltpu.VMEM((n_chip, 2, lanes), F32)] * n_blk,
+                [pltpu.VMEM((rows, LANES), F32)] * n_blk,
                 pltpu.VMEM((n_blk, 2, lanes), BF16),
                 pltpu.VMEM((n_sp, n_blk, 2, lanes), BF16),
                 pltpu.VMEM((n_blk, 8, lanes), F32),
@@ -516,6 +552,7 @@
                 dma((n_tp,)),
                 dma((n_tp,)),
                 pltpu.SemaphoreType.REGULAR((n_sp,)),
+                pltpu.SemaphoreType.REGULAR((n_tp,)),
             ],
             compiler_params=pltpu.CompilerParams(collective_id=0, has_side_effects=True),
         )(

time: 22.5 us -> 20.2 us (0.90)
  Pallas kernels: 21.7 us -> 19.3 us
    pallas_call x1, Pallas kernels: 21.7 us -> 19.3 us  [on_device(): pl.pallas_call(functools.partial(layer, n_sp, n_tp, state, group), out_sh...]
where the time goes in v2:
time: 20.2 us; the launch traced here: 20 us
  Pallas kernels  19.3 us (96%)
  local copies, waits for them, and re-layouts  0.68 us (3%)
    pallas_call x1, Pallas kernels, on_device(): pl.pallas_call(functools.partial(layer, n_sp, n_tp, state, group), out_sh...  19.3 us
    unnamed x1, local copies, waits for them, and re-layouts  0.68 us

profile of v2, /device:TPU:24, one launch (start us, length us, event | category | flops | bytes accessed | tf_op | source)
XLA Modules:
  0.0 20.0 jit_solution(17817353239248150874)
XLA Ops:
  0.0 19.3 %shard_map.118 = bf16[192,512]{1,0:T(8,128)(2,1)S(1)} custom-call(bf16[48,2048]{1,0:T(8,128)(2,1)} %tok_h.1, f32[1,2048]{1,0:T(1,128)} %bitcast.15, f32[32,64]{1,0:T(8,128)} %dlog_h.1, f32[32,64]{1,0:T(8,128)} %phase_h.1, f32[512,64]{1,0:T(8,128)} %bitcast.11, f32[512,64]{1,0:T(8,128)} %bitcast.12, f32[512,64]{1,0:T(8,128)} %bitcast.13, f32[512,64]{1,0:T(8,128)} %bitcast.14, ...), custom_call_target="tpu_custom_call" | custom-call | tf_op jit(solution)/shard_map/pallas_call | solution.py:505
  19.4 0.7 %copy.14 = bf16[192,512]{1,0:T(8,128)(2,1)} copy(bf16[192,512]{1,0:T(8,128)(2,1)S(1)} %shard_map.118) | data formatting | bytes 393216

commit v3 on v2

--- a/solution.py
+++ b/solution.py
@@ -44,9 +44,9 @@
     tok_h, nin_h, dlog_h, phase_h, bre_h, bim_h, cre_h, cim_h, skip_h, wv_h, wg_h, nout_h,
     out,
     nsend, urecv, rows_a, rows_p, t1r, t1i, t2r, t2i, bs, cs, wbuf, xbuf, wsum, ylocal,
-    e_send, e_all, l_ref, zbuf, wv, wg, acc_v, acc_g, sq_all,
-    bre, bim, cre, cim, tok, nin, dlog, phase, skip, nout,
-    load_sem, a_send, a_recv, e_ssem, e_rsem, z_send, z_recv, f_send, q_send, q_recv, met, met_tp,
+    e_send, e_all, l_ref, zbuf, w, acc_v, acc_g, sq_all,
+    bc, tok, nin, ap, sn,
+    load_sem, a_send, a_recv, e_ssem, e_rsem, z_send, z_recv, f_send, q_sem, met,
 ):
     sp, tp = lax.axis_index("sp"), lax.axis_index("tp")
     mine, d_model = tok.shape
@@ -62,18 +62,29 @@
     pair = 2 if n_sp % 2 == 0 else 1
     sp_b = lax.rem(sp, pair)
 
+    def load(i, *pairs):
+        return [pltpu.make_async_copy(src, dst, load_sem.at[i]) for src, dst in pairs]
+
     loads = [
-        pltpu.make_async_copy(src, dst, load_sem.at[i])
-        for i, (src, dst) in enumerate(
-            (
-                (tok_h, tok), (nin_h, nin), (dlog_h, dlog), (phase_h, phase),
-                (bre_h, bre), (bim_h, bim), (cre_h, cre), (cim_h, cim),
-                (skip_h, skip), (nout_h, nout), (wv_h, wv), (wg_h, wg),
-            )
-        )
+        load(0, (tok_h, tok)),
+        load(1, (nin_h, nin)),
+        load(2, (dlog_h, ap.at[0]), (phase_h, ap.at[1])),
+        load(3, *((src, bc.at[i]) for i, src in enumerate((bre_h, bim_h, cre_h, cim_h)))),
+        load(4, (skip_h, sn.at[0]), (nout_h, sn.at[1])),
+        load(5, (wv_h, w.at[0]), (wg_h, w.at[1])),
     ]
-    for copy in loads[:4]:
-        copy.start()
+
+    def start(*which):
+        for i in which:
+            for copy in loads[i]:
+                copy.start()
+
+    def loaded(*which):
+        for i in which:
+            dst = (tok, nin, ap, bc, sn, w)[i]
+            pltpu.make_async_copy(dst, dst, load_sem.at[i]).wait()
+
+    start(0, 1, 2)
 
     barrier = pltpu.get_barrier_semaphore()
 
@@ -97,13 +108,12 @@
 
     lax.fori_loop(tp + 1, n_tp, tell(barrier, "tp"), 0)
     above(tell(barrier, "sp"))
-    for copy in loads[4:10]:
-        copy.start()
+    start(3, 4)
     pl.when(tp + sp > 0)(lambda: pl.semaphore_wait(barrier, tp + (sp // pair + 1) * (sp_b + 1) - 1))
-    below(tell(met.at[sp], "sp"))
-    lax.fori_loop(0, tp, tell(met_tp.at[tp], "tp"), 0)
-    for copy in loads[:2]:
-        copy.wait()
+    half = (n_sp // 2 + pair - 1) // pair * pair
+    below(lambda j, c: tell(met.at[jnp.where(sp - j > half, 1, 0)], "sp")(j, c))
+    lax.fori_loop(0, tp, tell(met.at[2], "tp"), 0)
+    loaded(0, 1)
 
     xf = tok[...].astype(F32)
     scale = lax.rsqrt(jnp.sum(xf * xf, axis=1, keepdims=True) / d_model + NORM_EPS)
@@ -113,41 +123,27 @@
             at = j * width + blk * LANES
             nsend[j, blk] = normed[:, at : at + LANES]
 
-    def meet(sem):
-        def go(j, c):
-            pl.semaphore_wait(sem.at[j], 1)
-            return c
-
-        return go
-
-    lax.fori_loop(tp + 1, n_tp, meet(met_tp), 0)
-
-    sends = []
-    far_peers = []
-    for k in range(1, n_chip):
-        other = lax.rem(chip + n_chip - k, n_chip)
-        far_peers += [2 * other + core, 2 * other + 1 - core]
-
-    def scatter(i, j, blk):
-        copy = remote(
-            nsend.at[j, blk], urecv.at[tp, blk], a_send.at[i, blk], a_recv.at[tp, blk], {"tp": j}
-        )
-        copy.start()
-        sends.append(copy)
+    pl.when(tp < n_tp - 1)(lambda: pl.semaphore_wait(met.at[2], n_tp - 1 - tp))
+
+
+    def scatter(j, blk, at):
+        remote(nsend.at[j, blk], urecv.at[tp, blk], a_send.at[0], a_recv.at[at], {"tp": j}).start()
 
     for blk in range(n_blk):
-        for i, j in enumerate(far_peers):
-            scatter(i, j, blk)
+        for k in range(1, n_chip):
+            other = lax.rem(chip + n_chip - k, n_chip)
+            for j in (2 * other + core, 2 * other + 1 - core):
+                scatter(j, blk, 1 + (k - 1) * n_blk + blk)
         if blk == 0:
             for b in range(n_blk):
-                scatter(n_tp - 2, partner, b)
-
-    for copy in loads[10:]:
-        copy.start()
+                scatter(partner, b, 0)
+    start(5)
     urecv[tp] = nsend[tp]
 
-    for copy in loads[2:4]:
-        copy.wait()
+    loaded(2)
+    dlog, phase, skip, nout = ap.at[0], ap.at[1], sn.at[0], sn.at[1]
+    bre, bim, cre, cim = (bc.at[i] for i in range(4))
+    wv, wg = w.at[0], w.at[1]
     side = LANES // state
     for i in range(width // group // side):
         cut = slice(i * LANES, (i + 1) * LANES)
@@ -194,8 +190,7 @@
         for k, value in enumerate((allr, alli, lr[0:1], li[0:1], wholer, wholei, endr, endi)):
             l_ref[blk, k : k + 1, :] = value
 
-    for copy in loads[4:10]:
-        copy.wait()
+    loaded(3, 4)
     keep_b = (
         lax.broadcasted_iota(jnp.int32, (LANES, lanes), 0) // group
         == lax.broadcasted_iota(jnp.int32, (LANES, lanes), 1) // state
@@ -236,10 +231,11 @@
         >= lax.broadcasted_iota(jnp.int32, (span, span), 1)
     ).astype(BF16)
 
-    def taken(j, blk):
-        remote(
-            nsend.at[j, blk], urecv.at[j, blk], a_send.at[0, blk], a_recv.at[j, blk], {"tp": partner}
-        ).wait_recv()
+    def landed(ref, sem):
+        remote(ref, ref, a_send.at[0], sem, {"tp": partner}).wait_recv()
+
+    def gone(ref, sem):
+        remote(ref, ref, sem, a_recv.at[0], {"tp": partner}).wait_send()
 
     def source(c, blk):
         return jnp.concatenate([urecv[2 * c + s, blk].astype(F32) for s in range(2)], axis=0)
@@ -264,9 +260,7 @@
         return held
 
     def end_copy(j, blk):
-        return remote(
-            e_send.at[blk], e_all.at[sp, blk], e_ssem.at[j, blk], e_rsem.at[sp, blk], {"sp": j}
-        )
+        return remote(e_send.at[blk], e_all.at[blk, sp], e_ssem.at[0], e_rsem.at[blk], {"sp": j})
 
     def scan(blk):
         cut = slice(blk * lanes, (blk + 1) * lanes)
@@ -288,8 +282,7 @@
             at = slice(c * span, (c + 1) * span)
             ylocal[blk][at] = y[at] + skip[:, ch] * source(c, blk)
 
-    for blk in range(n_blk):
-        taken(partner, blk)
+    landed(urecv.at[partner], a_recv.at[0])
     for blk in range(n_blk):
         drive(chip, blk)
 
@@ -311,31 +304,28 @@
         for copy in z_copies(blk):
             copy.start()
 
+    def z_slot(k, blk, late):
+        return 1 + ((k - 1) * n_blk + blk) * 2 + late if k else 0
+
     def z_copies(blk):
         return [
             remote(
-                zbuf.at[tp, blk], zbuf.at[tp, blk], z_send.at[k, blk], z_recv.at[tp, blk],
+                zbuf.at[tp, blk], zbuf.at[tp, blk], z_send.at[0], z_recv.at[z_slot(k, blk, 0)],
                 {"tp": lax.rem(tp + 2 * k, n_tp) if k else partner},
             )
             for k in list(range(1, n_chip)) + [0]
         ]
 
-    def reach(j, c):
-        odd = lax.rem(j, pair)
-
-        @pl.when((sp_b == 0) | (odd == 0))
-        def _():
-            pl.semaphore_wait(met.at[jnp.where(sp_b == 0, j, j - odd + pair - 1)], 1)
-
-        return c
+    def reach(i, old, new):
+        count = new - old if pair == 1 else jnp.where(sp_b == 0, new - old, (new - old) // pair)
+        pl.when(count > 0)(lambda: pl.semaphore_wait(met.at[i], count))
 
     old = sp + 1
     for blk in range(n_blk + 2):
         if blk < n_blk:
             for k in range(1, n_chip):
                 c = lax.rem(chip + k, n_chip)
-                taken(2 * c, blk)
-                taken(2 * c + 1, blk)
+                landed(urecv.at[pl.ds(2 * c, 2), blk], a_recv.at[1 + (k - 1) * n_blk + blk])
             for k in range(1, n_chip):
                 drive(lax.rem(chip + k, n_chip), blk)
         if 1 <= blk <= n_blk:
@@ -345,8 +335,9 @@
         if blk < n_blk:
             er, ei = seeds(blk)[n_chip]
             e_send[blk] = jnp.concatenate([er, ei], axis=0).astype(BF16)
-            new = jnp.minimum(sp + 1 + n_sp // 2, n_sp) if blk == 0 else n_sp
-            lax.fori_loop(old, new, reach, 0)
+            new = jnp.minimum(sp + 1 + half, n_sp) if blk == 0 else n_sp
+            if blk < 2:
+                reach(blk, old, new)
             if blk:
                 send_ends([blk], sp + 1, old)
             send_ends(range(blk + 1), old, new)
@@ -359,13 +350,12 @@
         lr, li = l_ref[blk, 0:1], l_ref[blk, 1:2]
 
         def join(j, held):
-            remote(
-                e_send.at[blk], e_all.at[j, blk], e_ssem.at[j, blk], e_rsem.at[j, blk], {"sp": j}
-            ).wait_recv()
-            e = e_all[j, blk].astype(F32)
+            e = e_all[blk, j].astype(F32)
             hr, hi = cmul(*held, lr, li)
             return hr + e[0:1], hi + e[1:2]
 
+        for s in range(1, n_sp):
+            pl.when(sp == s)(functools.partial(landed, e_all.at[blk, pl.ds(0, s)], e_rsem.at[blk]))
         nil = jnp.zeros((1, lanes), F32)
         hr, hi = lax.fori_loop(0, sp, join, (nil, nil))
         hr, hi = cmul(hr, hi, l_ref[blk, 2:3], l_ref[blk, 3:4])
@@ -379,13 +369,7 @@
         for blk in range(n_blk):
             after(blk)
 
-    for copy in loads[10:]:
-        copy.wait()
-
-    def arrived(j, blk):
-        remote(
-            zbuf.at[j, blk], zbuf.at[j, blk], z_send.at[0, blk], z_recv.at[j, blk], {"tp": partner}
-        ).wait_recv()
+    loaded(5)
 
     def project(items):
         at = [pl.ds(pl.multiple_of(j * width + blk * LANES, LANES), LANES) for j, blk in items]
@@ -397,8 +381,7 @@
 
     v, g = project([(tp, blk) for blk in range(n_blk)])
     acc_v[...], acc_g[...] = v, g
-    for blk in range(n_blk):
-        arrived(partner, blk)
+    landed(zbuf.at[partner], z_recv.at[0])
     v, g = project([(partner, blk) for blk in range(n_blk)])
     acc_v[...] += v
     acc_g[...] += g
@@ -414,28 +397,26 @@
     for blk in range(n_blk):
         for k in range(1, n_chip):
             j = lax.rem(tp + n_tp - 2 * k, n_tp)
-            arrived(j, blk)
-            copy = remote(
-                zbuf.at[j, blk], zbuf.at[j, blk], f_send.at[k, blk], z_recv.at[j, blk], {"tp": partner}
-            )
-            copy.start()
-            sends.append(copy)
+            landed(zbuf.at[j, blk], z_recv.at[z_slot(k, blk, 0)])
+            remote(
+                zbuf.at[j, blk], zbuf.at[j, blk], f_send.at[0], z_recv.at[z_slot(k, blk, 1)], {"tp": partner}
+            ).start()
             ripe.append((j, blk))
             if len(ripe) == 2:
                 flush()
-            late.append((lax.rem(partner + n_tp - 2 * k, n_tp), blk))
+            late.append((lax.rem(partner + n_tp - 2 * k, n_tp), blk, k))
             if len(late) > 1:
                 item = late.pop(0)
-                arrived(*item)
-                ripe.append(item)
+                landed(zbuf.at[item[0], item[1]], z_recv.at[z_slot(item[2], item[1], 1)])
+                ripe.append(item[:2])
                 if len(ripe) == 2:
                     flush()
     if ripe:
         flush()
     for item in late:
-        arrived(*item)
+        landed(zbuf.at[item[0], item[1]], z_recv.at[z_slot(item[2], item[1], 1)])
     if late:
-        v, g = project(late)
+        v, g = project([item[:2] for item in late])
         v, g = acc_v[...] + v, acc_g[...] + g
     else:
         v, g = acc_v[...], acc_g[...]
@@ -452,27 +433,18 @@
     for k in range(rows // 8):
         total = jnp.where(lane == k, sums[8 * k : 8 * k + 8], total)
     sq_all[tp] = total
-    sums_out = []
     for k in range(1, n_tp):
         j = lax.rem(tp + n_tp - k, n_tp)
-        copy = remote(sq_all.at[tp], sq_all.at[tp], q_send.at[k], q_recv.at[tp], {"tp": j})
-        copy.start()
-        sums_out.append(copy)
-    for blk in range(n_blk):
-        sends += z_copies(blk)
-    for copy in sends:
-        copy.wait_send()
-
-    def sent(j, c):
-        for blk in range(n_blk):
-            end_copy(j, blk).wait_send()
-        return c
-
-    lax.fori_loop(sp + 1, n_sp, sent, 0)
+        remote(sq_all.at[tp], sq_all.at[tp], q_sem.at[0], q_sem.at[1], {"tp": j}).start()
+    gone(nsend.at[pl.ds(0, n_tp - 1)], a_send.at[0])
+    gone(zbuf.at[pl.ds(0, n_chip)], z_send.at[0])
+    if n_chip > 1:
+        gone(zbuf.at[pl.ds(0, n_chip - 1)], f_send.at[0])
+    for s in range(n_sp - 1):
+        pl.when(sp == s)(functools.partial(gone, e_all.at[:, pl.ds(0, n_sp - 1 - s)], e_ssem.at[0]))
+    landed(sq_all.at[pl.ds(0, n_tp - 1)], q_sem.at[1])
     for k in range(1, n_tp):
-        j = lax.rem(tp + k, n_tp)
-        remote(sq_all.at[j], sq_all.at[j], q_send.at[k], q_recv.at[j], {"tp": j}).wait_recv()
-        total = total + sq_all[j]
+        total = total + sq_all[lax.rem(tp + k, n_tp)]
     scale = lax.rsqrt(total / d_model + NORM_EPS)
     for k in range(0, rows // 8, 2):
         two = range(k, min(k + 2, rows // 8))
@@ -480,8 +452,7 @@
         at = slice(8 * k, 8 * k + 8 * len(two))
         out[at, :] = (acc_v[at, :] * column * nout[...]).astype(BF16)
 
-    for copy in sums_out:
-        copy.wait_send()
+    gone(sq_all.at[pl.ds(0, n_tp - 1)], q_sem.at[0])
 
 
 def solution(mesh):
@@ -523,36 +494,28 @@
                 [pltpu.VMEM((n_chip, 2, lanes), F32)] * n_blk,
                 [pltpu.VMEM((rows, LANES), F32)] * n_blk,
                 pltpu.VMEM((n_blk, 2, lanes), BF16),
-                pltpu.VMEM((n_sp, n_blk, 2, lanes), BF16),
+                pltpu.VMEM((n_blk, n_sp, 2, lanes), BF16),
                 pltpu.VMEM((n_blk, 8, lanes), F32),
                 pltpu.VMEM((n_tp, n_blk, rows, LANES), BF16),
-                pltpu.VMEM(w_value.shape, BF16),
-                pltpu.VMEM(w_gate.shape, BF16),
+                pltpu.VMEM((2,) + w_value.shape, BF16),
                 pltpu.VMEM((rows, width), F32),
                 pltpu.VMEM((rows, width), F32),
                 pltpu.VMEM((n_tp, 8, LANES), F32),
-                pltpu.VMEM((width, state), F32),
-                pltpu.VMEM((width, state), F32),
-                pltpu.VMEM((width, state), F32),
-                pltpu.VMEM((width, state), F32),
+                pltpu.VMEM((4, width, state), F32),
                 pltpu.VMEM((mine, d_model), BF16),
                 pltpu.VMEM((1, d_model), F32),
-                pltpu.VMEM((groups, state), F32),
-                pltpu.VMEM((groups, state), F32),
-                pltpu.VMEM((1, width), F32),
-                pltpu.VMEM((1, width), F32),
-                dma((12,)),
-                dma((n_tp - 1, n_blk)),
-                dma((n_tp, n_blk)),
-                dma((n_sp, n_blk)),
-                dma((n_sp, n_blk)),
-                dma((n_chip, n_blk)),
-                dma((n_tp, n_blk)),
-                dma((n_chip, n_blk)),
-                dma((n_tp,)),
-                dma((n_tp,)),
-                pltpu.SemaphoreType.REGULAR((n_sp,)),
-                pltpu.SemaphoreType.REGULAR((n_tp,)),
+                pltpu.VMEM((2, groups, state), F32),
+                pltpu.VMEM((2, 1, width), F32),
+                dma((6,)),
+                dma((1,)),
+                dma((1 + (n_chip - 1) * n_blk,)),
+                dma((1,)),
+                dma((n_blk,)),
+                dma((1,)),
+                dma((1 + (n_chip - 1) * n_blk * 2,)),
+                dma((1,)),
+                dma((2,)),
+                pltpu.SemaphoreType.REGULAR((3,)),
             ],
             compiler_params=pltpu.CompilerParams(collective_id=0, has_side_effects=True),
         )(

time: 20.2 us -> 19.1 us (0.946)
  Pallas kernels: 19.3 us -> 18.1 us
    pallas_call x1, Pallas kernels: 19.3 us -> 18.1 us  [on_device(): pl.pallas_call(functools.partial(layer, n_sp, n_tp, state, group), out_sh...]
where the time goes in v3:
time: 19.1 us; the launch traced here: 18.8 us
  Pallas kernels  18.1 us (95%)
  local copies, waits for them, and re-layouts  0.68 us (4%)
    pallas_call x1, Pallas kernels, on_device(): pl.pallas_call(functools.partial(layer, n_sp, n_tp, state, group), out_sh...  18.1 us
    unnamed x1, local copies, waits for them, and re-layouts  0.68 us

profile of v3, /device:TPU:24, one launch (start us, length us, event | category | flops | bytes accessed | tf_op | source)
XLA Modules:
  0.0 18.8 jit_solution(5340421315508665556)
XLA Ops:
  0.0 18.1 %shard_map.118 = bf16[192,512]{1,0:T(8,128)(2,1)S(1)} custom-call(bf16[48,2048]{1,0:T(8,128)(2,1)} %tok_h.1, f32[1,2048]{1,0:T(1,128)} %bitcast.15, f32[32,64]{1,0:T(8,128)} %dlog_h.1, f32[32,64]{1,0:T(8,128)} %phase_h.1, f32[512,64]{1,0:T(8,128)} %bitcast.11, f32[512,64]{1,0:T(8,128)} %bitcast.12, f32[512,64]{1,0:T(8,128)} %bitcast.13, f32[512,64]{1,0:T(8,128)} %bitcast.14, ...), custom_call_target="tpu_custom_call" | custom-call | tf_op jit(solution)/shard_map/pallas_call | solution.py:476
  18.1 0.7 %copy.14 = bf16[192,512]{1,0:T(8,128)(2,1)} copy(bf16[192,512]{1,0:T(8,128)(2,1)S(1)} %shard_map.118) | data formatting | bytes 393216

commit v4 on v3

--- a/solution.py
+++ b/solution.py
@@ -44,13 +44,14 @@
     tok_h, nin_h, dlog_h, phase_h, bre_h, bim_h, cre_h, cim_h, skip_h, wv_h, wg_h, nout_h,
     out,
     nsend, urecv, rows_a, rows_p, t1r, t1i, t2r, t2i, bs, cs, wbuf, xbuf, wsum, ylocal,
-    e_send, e_all, l_ref, zbuf, w, acc_v, acc_g, sq_all,
+    e_send, e_all, l_ref, zst, zbuf, w, acc, both, swapped, sq_all,
     bc, tok, nin, ap, sn,
-    load_sem, a_send, a_recv, e_ssem, e_rsem, z_send, z_recv, f_send, q_sem, met,
+    load_sem, a_send, a_recv, e_ssem, e_rsem, z_send, z_recv, w_sem, q_sem, met,
 ):
     sp, tp = lax.axis_index("sp"), lax.axis_index("tp")
     mine, d_model = tok.shape
-    rows, width = acc_v.shape
+    rows, width = out.shape
+    half_rows = rows // 2
     n_blk = width // LANES
     per = LANES // group
     lanes = per * state
@@ -71,7 +72,7 @@
         load(2, (dlog_h, ap.at[0]), (phase_h, ap.at[1])),
         load(3, *((src, bc.at[i]) for i, src in enumerate((bre_h, bim_h, cre_h, cim_h)))),
         load(4, (skip_h, sn.at[0]), (nout_h, sn.at[1])),
-        load(5, (wv_h, w.at[0]), (wg_h, w.at[1])),
+        load(5, (wv_h, w.at[core, 0]), (wg_h, w.at[core, 1])),
     ]
 
     def start(*which):
@@ -81,7 +82,7 @@
 
     def loaded(*which):
         for i in which:
-            dst = (tok, nin, ap, bc, sn, w)[i]
+            dst = (tok, nin, ap, bc, sn, w.at[core])[i]
             pltpu.make_async_copy(dst, dst, load_sem.at[i]).wait()
 
     start(0, 1, 2)
@@ -138,12 +139,13 @@
             for b in range(n_blk):
                 scatter(partner, b, 0)
     start(5)
+    for i, src in enumerate((wv_h, wg_h)):
+        remote(src, w.at[core, i], w_sem.at[0], w_sem.at[1], {"tp": partner}).start()
     urecv[tp] = nsend[tp]
 
     loaded(2)
     dlog, phase, skip, nout = ap.at[0], ap.at[1], sn.at[0], sn.at[1]
     bre, bim, cre, cim = (bc.at[i] for i in range(4))
-    wv, wg = w.at[0], w.at[1]
     side = LANES // state
     for i in range(width // group // side):
         cut = slice(i * LANES, (i + 1) * LANES)
@@ -300,20 +302,21 @@
             v = ylocal[blk][at]
             if y is not None:
                 v = v + y[:, c * LANES : (c + 1) * LANES]
-            zbuf[tp, blk, at] = jax.nn.gelu(v).astype(BF16)
+            top = c * span // half_rows
+            to = slice(c * span - top * half_rows, (c + 1) * span - top * half_rows)
+            zst[top, blk, to] = jax.nn.gelu(v).astype(BF16)
         for copy in z_copies(blk):
             copy.start()
 
-    def z_slot(k, blk, late):
-        return 1 + ((k - 1) * n_blk + blk) * 2 + late if k else 0
-
     def z_copies(blk):
+        targets = []
+        for k in range(1, n_chip):
+            other = 2 * lax.rem(chip + k, n_chip)
+            targets += [(h, other + h, 1 + (k - 1) * n_blk + blk) for h in (core, 1 - core)]
+        targets.append((1 - core, partner, 0))
         return [
-            remote(
-                zbuf.at[tp, blk], zbuf.at[tp, blk], z_send.at[0], z_recv.at[z_slot(k, blk, 0)],
-                {"tp": lax.rem(tp + 2 * k, n_tp) if k else partner},
-            )
-            for k in list(range(1, n_chip)) + [0]
+            remote(zst.at[h, blk], zbuf.at[tp, blk], z_send.at[0], z_recv.at[slot], {"tp": j})
+            for h, j, slot in targets
         ]
 
     def reach(i, old, new):
@@ -371,88 +374,81 @@
 
     loaded(5)
 
-    def project(items):
-        at = [pl.ds(pl.multiple_of(j * width + blk * LANES, LANES), LANES) for j, blk in items]
-        z = jnp.concatenate([zbuf[j, blk] for j, blk in items], axis=1)
+    def project(ref, i, j, blks):
+        at = pl.ds(pl.multiple_of(j * width + blks[0] * LANES, LANES), LANES * len(blks))
+        z = jnp.concatenate([ref[i, blk] for blk in blks], axis=1)
+        return z, at
+
+    def products(*parts):
+        z = jnp.concatenate([p[0] for p in parts], axis=1)
         return [
-            jnp.dot(z, jnp.concatenate([w[a, :] for a in at], axis=0), preferred_element_type=F32)
-            for w in (wv, wg)
+            [
+                jnp.dot(
+                    z, jnp.concatenate([w[q, i, p[1], :] for p in parts], axis=0), preferred_element_type=F32
+                )
+                for i in range(2)
+            ]
+            for q in range(2)
         ]
 
-    v, g = project([(tp, blk) for blk in range(n_blk)])
-    acc_v[...], acc_g[...] = v, g
+    def add(new):
+        for q in range(2):
+            for i in range(2):
+                acc[q, i] += new[q][i]
+
+    landed(w.at[1 - core], w_sem.at[1])
+    every = range(n_blk)
+    new = products(project(zst, core, tp, every))
+    for q in range(2):
+        for i in range(2):
+            acc[q, i] = new[q][i]
     landed(zbuf.at[partner], z_recv.at[0])
-    v, g = project([(partner, blk) for blk in range(n_blk)])
-    acc_v[...] += v
-    acc_g[...] += g
-    late = []
-    ripe = []
-
-    def flush():
-        v, g = project(ripe)
-        ripe.clear()
-        acc_v[...] += v
-        acc_g[...] += g
-
+    add(products(project(zbuf, partner, partner, every)))
     for blk in range(n_blk):
         for k in range(1, n_chip):
-            j = lax.rem(tp + n_tp - 2 * k, n_tp)
-            landed(zbuf.at[j, blk], z_recv.at[z_slot(k, blk, 0)])
-            remote(
-                zbuf.at[j, blk], zbuf.at[j, blk], f_send.at[0], z_recv.at[z_slot(k, blk, 1)], {"tp": partner}
-            ).start()
-            ripe.append((j, blk))
-            if len(ripe) == 2:
-                flush()
-            late.append((lax.rem(partner + n_tp - 2 * k, n_tp), blk, k))
-            if len(late) > 1:
-                item = late.pop(0)
-                landed(zbuf.at[item[0], item[1]], z_recv.at[z_slot(item[2], item[1], 1)])
-                ripe.append(item[:2])
-                if len(ripe) == 2:
-                    flush()
-    if ripe:
-        flush()
-    for item in late:
-        landed(zbuf.at[item[0], item[1]], z_recv.at[z_slot(item[2], item[1], 1)])
-    if late:
-        v, g = project([item[:2] for item in late])
-        v, g = acc_v[...] + v, acc_g[...] + g
-    else:
-        v, g = acc_v[...], acc_g[...]
-
-    gated = v * (0.5 + 0.5 * jnp.tanh(0.5 * g))
-    acc_v[...] = gated
-    square = gated * gated
-    part = square[:, :LANES]
-    for blk in range(1, n_blk):
-        part = part + square[:, blk * LANES : (blk + 1) * LANES]
+            c2 = 2 * lax.rem(chip + n_chip - k, n_chip)
+            landed(zbuf.at[pl.ds(c2, 2), blk], z_recv.at[1 + (k - 1) * n_blk + blk])
+            new = products(*(project(zbuf, c2 + h, c2 + h, [blk]) for h in range(2)))
+            if blk < n_blk - 1 or k < n_chip - 1:
+                add(new)
+    part = None
+    for q in range(2):
+        v, g = (acc[q, i] + new[q][i] for i in range(2))
+        gated = v * (0.5 + 0.5 * jnp.tanh(0.5 * g))
+        both[q] = gated
+        square = gated * gated
+        for blk in range(n_blk):
+            piece = square[:, blk * LANES : (blk + 1) * LANES]
+            part = piece if part is None else part + piece
+    remote(both.at[1 - core], swapped, q_sem.at[2], q_sem.at[3], {"tp": partner}).start()
     sums = jnp.sum(part, axis=1, keepdims=True)
     lane = lax.broadcasted_iota(jnp.int32, (8, LANES), 1)
     total = jnp.zeros((8, LANES), F32)
-    for k in range(rows // 8):
+    for k in range(half_rows // 8):
         total = jnp.where(lane == k, sums[8 * k : 8 * k + 8], total)
     sq_all[tp] = total
     for k in range(1, n_tp):
         j = lax.rem(tp + n_tp - k, n_tp)
         remote(sq_all.at[tp], sq_all.at[tp], q_sem.at[0], q_sem.at[1], {"tp": j}).start()
     gone(nsend.at[pl.ds(0, n_tp - 1)], a_send.at[0])
-    gone(zbuf.at[pl.ds(0, n_chip)], z_send.at[0])
-    if n_chip > 1:
-        gone(zbuf.at[pl.ds(0, n_chip - 1)], f_send.at[0])
+    gone(zbuf.at[pl.ds(0, n_tp - 1)], z_send.at[0])
+    gone(w.at[core], w_sem.at[0])
     for s in range(n_sp - 1):
         pl.when(sp == s)(functools.partial(gone, e_all.at[:, pl.ds(0, n_sp - 1 - s)], e_ssem.at[0]))
     landed(sq_all.at[pl.ds(0, n_tp - 1)], q_sem.at[1])
-    for k in range(1, n_tp):
-        total = total + sq_all[lax.rem(tp + k, n_tp)]
-    scale = lax.rsqrt(total / d_model + NORM_EPS)
-    for k in range(0, rows // 8, 2):
-        two = range(k, min(k + 2, rows // 8))
-        column = jnp.concatenate([scale[:, i : i + 1] for i in two], axis=0)
-        at = slice(8 * k, 8 * k + 8 * len(two))
-        out[at, :] = (acc_v[at, :] * column * nout[...]).astype(BF16)
+    landed(swapped, q_sem.at[3])
+    for h in (core, 1 - core):
+        total = sq_all[h]
+        for c in range(1, n_chip):
+            total = total + sq_all[2 * c + h]
+        scale = lax.rsqrt(total / d_model + NORM_EPS)
+        column = jnp.concatenate([scale[:, i : i + 1] for i in range(half_rows // 8)], axis=0)
+        gated = both[core] if h is core else swapped[...]
+        at = pl.ds(pl.multiple_of(h * half_rows, half_rows), half_rows)
+        out[at, :] = (gated * column * nout[...]).astype(BF16)
 
     gone(sq_all.at[pl.ds(0, n_tp - 1)], q_sem.at[0])
+    gone(swapped, q_sem.at[2])
 
 
 def solution(mesh):
@@ -496,10 +492,12 @@
                 pltpu.VMEM((n_blk, 2, lanes), BF16),
                 pltpu.VMEM((n_blk, n_sp, 2, lanes), BF16),
                 pltpu.VMEM((n_blk, 8, lanes), F32),
-                pltpu.VMEM((n_tp, n_blk, rows, LANES), BF16),
-                pltpu.VMEM((2,) + w_value.shape, BF16),
-                pltpu.VMEM((rows, width), F32),
-                pltpu.VMEM((rows, width), F32),
+                pltpu.VMEM((2, n_blk, rows // 2, LANES), BF16),
+                pltpu.VMEM((n_tp, n_blk, rows // 2, LANES), BF16),
+                pltpu.VMEM((2, 2) + w_value.shape, BF16),
+                pltpu.VMEM((2, 2, rows // 2, width), F32),
+                pltpu.VMEM((2, rows // 2, width), F32),
+                pltpu.VMEM((rows // 2, width), F32),
                 pltpu.VMEM((n_tp, 8, LANES), F32),
                 pltpu.VMEM((4, width, state), F32),
                 pltpu.VMEM((mine, d_model), BF16),
@@ -512,9 +510,9 @@
                 dma((1,)),
                 dma((n_blk,)),
                 dma((1,)),
-                dma((1 + (n_chip - 1) * n_blk * 2,)),
-                dma((1,)),
+                dma((1 + (n_chip - 1) * n_blk,)),
                 dma((2,)),
+                dma((4,)),
                 pltpu.SemaphoreType.REGULAR((3,)),
             ],
             compiler_params=pltpu.CompilerParams(collective_id=0, has_side_effects=True),

time: 19.1 us -> 18 us (0.942)
  Pallas kernels: 18.1 us -> 17 us
    pallas_call x1, Pallas kernels: 18.1 us -> 17 us  [on_device(): pl.pallas_call(functools.partial(layer, n_sp, n_tp, state, group), out_sh...]
where the time goes in v4:
time: 18 us; the launch traced here: 17.7 us
  Pallas kernels  17 us (94%)
  local copies, waits for them, and re-layouts  0.68 us (4%)
    pallas_call x1, Pallas kernels, on_device(): pl.pallas_call(functools.partial(layer, n_sp, n_tp, state, group), out_sh...  17 us
    unnamed x1, local copies, waits for them, and re-layouts  0.68 us

profile of v4, /device:TPU:24, one launch (start us, length us, event | category | flops | bytes accessed | tf_op | source)
XLA Modules:
  0.0 17.7 jit_solution(9633204806256412454)
XLA Ops:
  0.0 17.0 %shard_map.118 = bf16[192,512]{1,0:T(8,128)(2,1)S(1)} custom-call(bf16[48,2048]{1,0:T(8,128)(2,1)} %tok_h.1, f32[1,2048]{1,0:T(1,128)} %bitcast.15, f32[32,64]{1,0:T(8,128)} %dlog_h.1, f32[32,64]{1,0:T(8,128)} %phase_h.1, f32[512,64]{1,0:T(8,128)} %bitcast.11, f32[512,64]{1,0:T(8,128)} %bitcast.12, f32[512,64]{1,0:T(8,128)} %bitcast.13, f32[512,64]{1,0:T(8,128)} %bitcast.14, ...), custom_call_target="tpu_custom_call" | custom-call | tf_op jit(solution)/shard_map/pallas_call | solution.py:472
  17.0 0.7 %copy.14 = bf16[192,512]{1,0:T(8,128)(2,1)} copy(bf16[192,512]{1,0:T(8,128)(2,1)S(1)} %shard_map.118) | data formatting | bytes 393216

commit v5 on v4

--- a/solution.py
+++ b/solution.py
@@ -63,11 +63,13 @@
     pair = 2 if n_sp % 2 == 0 else 1
     sp_b = lax.rem(sp, pair)
 
+    parts = [pl.ds(i * width, width) for i in range(n_tp)]
+
     def load(i, *pairs):
         return [pltpu.make_async_copy(src, dst, load_sem.at[i]) for src, dst in pairs]
 
     loads = [
-        load(0, (tok_h, tok)),
+        load(0, *((tok_h.at[:, part], tok.at[:, part]) for part in parts)),
         load(1, (nin_h, nin)),
         load(2, (dlog_h, ap.at[0]), (phase_h, ap.at[1])),
         load(3, *((src, bc.at[i]) for i, src in enumerate((bre_h, bim_h, cre_h, cim_h)))),
@@ -107,13 +109,20 @@
             last = sp // pair + jnp.where(b < sp_b, 1, 0)
             lax.fori_loop(0, jnp.where(b <= sp_b, last, 0), lambda a, c, b=b: go(a * pair + b, c), 0)
 
+    last = sp == n_sp - 1
+    lax.fori_loop(jnp.where(last, tp + 1, 0), jnp.where(last, tp + 1, tp), tell(barrier, "tp"), 0)
     lax.fori_loop(tp + 1, n_tp, tell(barrier, "tp"), 0)
     above(tell(barrier, "sp"))
     start(3, 4)
-    pl.when(tp + sp > 0)(lambda: pl.semaphore_wait(barrier, tp + (sp // pair + 1) * (sp_b + 1) - 1))
+    known = (sp // pair + 1) * (sp_b + 1) - 1 + jnp.where(last, tp, n_tp - 1)
     half = (n_sp // 2 + pair - 1) // pair * pair
-    below(lambda j, c: tell(met.at[jnp.where(sp - j > half, 1, 0)], "sp")(j, c))
-    lax.fori_loop(0, tp, tell(met.at[2], "tp"), 0)
+
+    def enter():
+        pl.when(known > 0)(lambda: pl.semaphore_wait(barrier, known))
+        below(lambda j, c: tell(met.at[jnp.where(sp - j > half, 1, 0)], "sp")(j, c))
+        lax.fori_loop(0, jnp.where(last, tp, 0), tell(met.at[2], "tp"), 0)
+
+    pl.when(last)(enter)
     loaded(0, 1)
 
     xf = tok[...].astype(F32)
@@ -124,7 +133,8 @@
             at = j * width + blk * LANES
             nsend[j, blk] = normed[:, at : at + LANES]
 
-    pl.when(tp < n_tp - 1)(lambda: pl.semaphore_wait(met.at[2], n_tp - 1 - tp))
+    pl.when(jnp.logical_not(last))(enter)
+    pl.when(last & (tp < n_tp - 1))(lambda: pl.semaphore_wait(met.at[2], n_tp - 1 - tp))
 
 
     def scatter(j, blk, at):
@@ -345,7 +355,15 @@
                 send_ends([blk], sp + 1, old)
             send_ends(range(blk + 1), old, new)
             old = new
-        if 2 <= blk:
+        if blk == 0:
+
+            @pl.when(sp == 0)
+            def _():
+                scan(0)
+                readout(0)
+                finish(0, None)
+
+        if 3 <= blk:
             pl.when(sp == 0)(functools.partial(finish, blk - 2, None))
 
     def after(blk):
@@ -435,8 +453,10 @@
     gone(w.at[core], w_sem.at[0])
     for s in range(n_sp - 1):
         pl.when(sp == s)(functools.partial(gone, e_all.at[:, pl.ds(0, n_sp - 1 - s)], e_ssem.at[0]))
+    both[core] = both[core] * nout[...]
+    landed(swapped, q_sem.at[3])
+    swapped[...] = swapped[...] * nout[...]
     landed(sq_all.at[pl.ds(0, n_tp - 1)], q_sem.at[1])
-    landed(swapped, q_sem.at[3])
     for h in (core, 1 - core):
         total = sq_all[h]
         for c in range(1, n_chip):
@@ -445,7 +465,7 @@
         column = jnp.concatenate([scale[:, i : i + 1] for i in range(half_rows // 8)], axis=0)
         gated = both[core] if h is core else swapped[...]
         at = pl.ds(pl.multiple_of(h * half_rows, half_rows), half_rows)
-        out[at, :] = (gated * column * nout[...]).astype(BF16)
+        out[at, :] = (gated * column).astype(BF16)
 
     gone(sq_all.at[pl.ds(0, n_tp - 1)], q_sem.at[0])
     gone(swapped, q_sem.at[2])

time: 18 us -> 17.8 us (0.989)
  no operation moved by 1% of the time
where the time goes in v5:
time: 17.8 us; the launch traced here: 17.7 us
  Pallas kernels  17 us (96%)
  local copies, waits for them, and re-layouts  0.68 us (4%)
    pallas_call x1, Pallas kernels, on_device(): pl.pallas_call(functools.partial(layer, n_sp, n_tp, state, group), out_sh...  17 us
    unnamed x1, local copies, waits for them, and re-layouts  0.68 us

profile of v5, /device:TPU:24, one launch (start us, length us, event | category | flops | bytes accessed | tf_op | source)
XLA Modules:
  0.0 17.7 jit_solution(6995744584849238464)
XLA Ops:
  0.0 17.0 %shard_map.118 = bf16[192,512]{1,0:T(8,128)(2,1)S(1)} custom-call(bf16[48,2048]{1,0:T(8,128)(2,1)} %tok_h.1, f32[1,2048]{1,0:T(1,128)} %bitcast.15, f32[32,64]{1,0:T(8,128)} %dlog_h.1, f32[32,64]{1,0:T(8,128)} %phase_h.1, f32[512,64]{1,0:T(8,128)} %bitcast.11, f32[512,64]{1,0:T(8,128)} %bitcast.12, f32[512,64]{1,0:T(8,128)} %bitcast.13, f32[512,64]{1,0:T(8,128)} %bitcast.14, ...), custom_call_target="tpu_custom_call" | custom-call | tf_op jit(solution)/shard_map/pallas_call | solution.py:492
  17.0 0.7 %copy.14 = bf16[192,512]{1,0:T(8,128)(2,1)} copy(bf16[192,512]{1,0:T(8,128)(2,1)S(1)} %shard_map.118) | data formatting | bytes 393216

commit v6 on v5

--- a/solution.py
+++ b/solution.py
@@ -44,9 +44,9 @@
     tok_h, nin_h, dlog_h, phase_h, bre_h, bim_h, cre_h, cim_h, skip_h, wv_h, wg_h, nout_h,
     out,
     nsend, urecv, rows_a, rows_p, t1r, t1i, t2r, t2i, bs, cs, wbuf, xbuf, wsum, ylocal,
-    e_send, e_all, l_ref, zst, zbuf, w, acc, both, swapped, sq_all,
+    e_send, e_all, l_ref, zst, zbuf, w, acc, both, swapped, sq_all, ct, xct, xcs, yst, lh, xlh,
     bc, tok, nin, ap, sn,
-    load_sem, a_send, a_recv, e_ssem, e_rsem, z_send, z_recv, w_sem, q_sem, met,
+    load_sem, a_send, a_recv, e_ssem, e_rsem, z_send, z_recv, w_sem, q_sem, c_sem, h_sem, met,
 ):
     sp, tp = lax.axis_index("sp"), lax.axis_index("tp")
     mine, d_model = tok.shape
@@ -62,6 +62,8 @@
     span = 2 * mine
     pair = 2 if n_sp % 2 == 0 else 1
     sp_b = lax.rem(sp, pair)
+    early = 0
+    half_chips = n_chip // 2
 
     parts = [pl.ds(i * width, width) for i in range(n_tp)]
 
@@ -211,6 +213,14 @@
     a, p = dlog[...], phase[...]
     mag = jnp.exp(a)
     stepr, stepi = cpow(mag * jnp.cos(p), mag * jnp.sin(p), span)
+
+    def widen(dst, turned, c):
+        for part in range(2):
+            piece = turned[part * state : (part + 1) * state]
+            for g in range(per):
+                at = part * lanes + g * state
+                dst[at : at + state, c * LANES : (c + 1) * LANES] = jnp.where(of_col == g, piece, 0.0).astype(BF16)
+
     for blk in range(n_blk):
         ch = slice(blk * LANES, (blk + 1) * LANES)
         for part, in_ref in ((0, bre), (1, bim)):
@@ -231,13 +241,22 @@
             if c:
                 c_r, c_i = cmul(c_r, c_i, *spread)
             turned = jnp.concatenate([c_r, -c_i], axis=1).T
-            for part in range(2):
-                piece = turned[part * state : (part + 1) * state]
-                for g in range(per):
-                    at = part * lanes + g * state
-                    cs[blk, at : at + state, c * LANES : (c + 1) * LANES] = jnp.where(
-                        of_col == g, piece, 0.0
-                    ).astype(BF16)
+            if blk == early:
+                ct[c] = turned.astype(BF16)
+            widen(cs.at[blk], turned, c)
+    def across(start):
+        for k in range(1, n_chip):
+            for h in range(2):
+                start(h, 2 * lax.rem(chip + k, n_chip) + h)
+
+    @pl.when(sp > 0)
+    def _():
+        across(
+            lambda h, j: remote(
+                ct.at[pl.ds(h * half_chips, half_chips)], xct.at[tp], c_sem.at[0], c_sem.at[1], {"tp": j}
+            ).start()
+        )
+
     lower = (
         lax.broadcasted_iota(jnp.int32, (span, span), 0)
         >= lax.broadcasted_iota(jnp.int32, (span, span), 1)
@@ -312,59 +331,86 @@
             v = ylocal[blk][at]
             if y is not None:
                 v = v + y[:, c * LANES : (c + 1) * LANES]
-            top = c * span // half_rows
-            to = slice(c * span - top * half_rows, (c + 1) * span - top * half_rows)
+            top, to = half_of(c)
             zst[top, blk, to] = jax.nn.gelu(v).astype(BF16)
-        for copy in z_copies(blk):
-            copy.start()
-
-    def z_copies(blk):
-        targets = []
+        if y is None or blk != early:
+            cross(blk, zst.at[:, blk])
+        remote(
+            zst.at[1 - core, blk], zbuf.at[tp, blk], z_send.at[0], z_recv.at[0], {"tp": partner}
+        ).start()
+
+    def half_of(c):
+        top = c * span // half_rows
+        return top, slice(c * span - top * half_rows, (c + 1) * span - top * half_rows)
+
+    def cross(blk, src):
         for k in range(1, n_chip):
-            other = 2 * lax.rem(chip + k, n_chip)
-            targets += [(h, other + h, 1 + (k - 1) * n_blk + blk) for h in (core, 1 - core)]
-        targets.append((1 - core, partner, 0))
-        return [
-            remote(zst.at[h, blk], zbuf.at[tp, blk], z_send.at[0], z_recv.at[slot], {"tp": j})
-            for h, j, slot in targets
-        ]
+            for h in (core, 1 - core):
+                remote(
+                    src.at[h], zbuf.at[tp, blk], z_send.at[0], z_recv.at[1 + (k - 1) * n_blk + blk],
+                    {"tp": 2 * lax.rem(chip + k, n_chip) + h},
+                ).start()
 
     def reach(i, old, new):
         count = new - old if pair == 1 else jnp.where(sp_b == 0, new - old, (new - old) // pair)
         pl.when(count > 0)(lambda: pl.semaphore_wait(met.at[i], count))
 
-    old = sp + 1
-    for blk in range(n_blk + 2):
-        if blk < n_blk:
-            for k in range(1, n_chip):
-                c = lax.rem(chip + k, n_chip)
-                landed(urecv.at[pl.ds(2 * c, 2), blk], a_recv.at[1 + (k - 1) * n_blk + blk])
-            for k in range(1, n_chip):
-                drive(lax.rem(chip + k, n_chip), blk)
-        if 1 <= blk <= n_blk:
-            scan(blk - 1)
-        if 2 <= blk:
-            readout(blk - 2)
-        if blk < n_blk:
-            er, ei = seeds(blk)[n_chip]
-            e_send[blk] = jnp.concatenate([er, ei], axis=0).astype(BF16)
-            new = jnp.minimum(sp + 1 + half, n_sp) if blk == 0 else n_sp
-            if blk < 2:
-                reach(blk, old, new)
-            if blk:
-                send_ends([blk], sp + 1, old)
-            send_ends(range(blk + 1), old, new)
-            old = new
+    def take(blk):
+        for k in range(1, n_chip):
+            c = lax.rem(chip + k, n_chip)
+            landed(urecv.at[pl.ds(2 * c, 2), blk], a_recv.at[1 + (k - 1) * n_blk + blk])
+        for k in range(1, n_chip):
+            drive(lax.rem(chip + k, n_chip), blk)
+
+    close = jnp.minimum(sp + 1 + half, n_sp)
+
+    def give(blk):
+        er, ei = seeds(blk)[n_chip]
+        e_send[blk] = jnp.concatenate([er, ei], axis=0).astype(BF16)
+
+    def post(blk):
         if blk == 0:
-
-            @pl.when(sp == 0)
-            def _():
-                scan(0)
-                readout(0)
-                finish(0, None)
-
-        if 3 <= blk:
-            pl.when(sp == 0)(functools.partial(finish, blk - 2, None))
+            reach(0, sp + 1, close)
+            send_ends([0], sp + 1, close)
+            return
+        if blk == 1:
+            reach(1, close, n_sp)
+        send_ends([blk], sp + 1, close)
+        send_ends(range(2) if blk == 1 else [blk], close, n_sp)
+
+    @pl.when(sp == 0)
+    def _():
+        for blk in range(n_blk):
+            take(blk)
+            give(blk)
+            if blk != 1:
+                post(blk)
+            else:
+                send_ends([1], sp + 1, close)
+            scan(blk)
+            readout(blk)
+            finish(blk, None)
+            if blk == 1:
+                reach(1, close, n_sp)
+                send_ends(range(2), close, n_sp)
+
+    @pl.when(sp > 0)
+    def _():
+        for blk in range(n_blk + 2):
+            if blk < n_blk:
+                take(blk)
+            if 1 <= blk <= n_blk:
+                scan(blk - 1)
+            if 2 <= blk:
+                readout(blk - 2)
+            if blk < n_blk:
+                give(blk)
+                post(blk)
+            if blk - 2 == early:
+                for c in range(n_chip):
+                    top, to = half_of(c)
+                    yst[top, to] = ylocal[early][c * span : (c + 1) * span].astype(BF16)
+                cross(early, yst)
 
     def after(blk):
         cut = slice(blk * lanes, (blk + 1) * lanes)
@@ -380,6 +426,9 @@
         nil = jnp.zeros((1, lanes), F32)
         hr, hi = lax.fori_loop(0, sp, join, (nil, nil))
         hr, hi = cmul(hr, hi, l_ref[blk, 2:3], l_ref[blk, 3:4])
+        if blk == early:
+            lh[...] = jnp.concatenate([l_ref[blk, 2:4], hr, hi], axis=0)
+            across(lambda h, j: remote(lh, xlh.at[tp], h_sem.at[0], h_sem.at[1], {"tp": j}).start())
         xr, xi = cmul(hr, hi, t2r[:, cut], t2i[:, cut])
         x = jnp.concatenate([xr.astype(BF16), xi.astype(BF16)], axis=1)
         finish(blk, jnp.dot(x, cs[blk], preferred_element_type=F32))
@@ -389,6 +438,43 @@
     def _():
         for blk in range(n_blk):
             after(blk)
+
+    @pl.when(sp > 0)
+    def _():
+        landed(xct.at[pl.ds(0, n_tp - 2)], c_sem.at[1])
+        for k in range(1, n_chip):
+            for h in range(2):
+                j = 2 * lax.rem(chip + n_chip - k, n_chip) + h
+                for c in range(half_chips):
+                    widen(xcs.at[2 * (k - 1) + h], xct[j, c].astype(F32), c)
+
+    def correct(k, c2):
+        if k == 1:
+            landed(xlh.at[pl.ds(0, n_tp - 2)], h_sem.at[1])
+        fixed = []
+        for h in range(2):
+            j = c2 + h
+            lr, li, pr, pi = (jnp.broadcast_to(xlh[j, i : i + 1], (8, lanes)) for i in range(4))
+            row = lax.broadcasted_iota(jnp.int32, (8, lanes), 0)
+            for bit in range(3):
+                on = lax.rem(row // (1 << bit), 2) == 1
+                ar, ai = cmul(pr, pi, lr, li)
+                pr, pi = jnp.where(on, ar, pr), jnp.where(on, ai, pi)
+                lr, li = cmul(lr, li, lr, li)
+            pieces = [(pr, pi)]
+            while len(pieces) < span // 8:
+                pieces += [cmul(*p, lr, li) for p in pieces[: span // 8 - len(pieces)]]
+                lr, li = cmul(lr, li, lr, li)
+            x = jnp.concatenate(
+                [jnp.concatenate([p[i] for p in pieces], axis=0).astype(BF16) for i in range(2)], axis=1
+            )
+            fixed.append(jnp.dot(x, xcs[2 * (k - 1) + h], preferred_element_type=F32))
+        held = [zbuf[c2 + h, early].astype(F32) for h in range(2)]
+        for h in range(2):
+            y = jnp.concatenate([fixed[h][:, c * LANES : (c + 1) * LANES] for c in range(half_chips)], axis=0)
+            held[h] = jax.nn.gelu(held[h] + y).astype(BF16)
+        for h in range(2):
+            zbuf[c2 + h, early] = held[h]
 
     loaded(5)
 
@@ -426,6 +512,8 @@
         for k in range(1, n_chip):
             c2 = 2 * lax.rem(chip + n_chip - k, n_chip)
             landed(zbuf.at[pl.ds(c2, 2), blk], z_recv.at[1 + (k - 1) * n_blk + blk])
+            if blk == early:
+                pl.when(sp > 0)(functools.partial(correct, k, c2))
             new = products(*(project(zbuf, c2 + h, c2 + h, [blk]) for h in range(2)))
             if blk < n_blk - 1 or k < n_chip - 1:
                 add(new)
@@ -451,6 +539,12 @@
     gone(nsend.at[pl.ds(0, n_tp - 1)], a_send.at[0])
     gone(zbuf.at[pl.ds(0, n_tp - 1)], z_send.at[0])
     gone(w.at[core], w_sem.at[0])
+
+    @pl.when(sp > 0)
+    def _():
+        gone(xct.at[pl.ds(0, n_tp - 2)], c_sem.at[0])
+        gone(xlh.at[pl.ds(0, n_tp - 2)], h_sem.at[0])
+
     for s in range(n_sp - 1):
         pl.when(sp == s)(functools.partial(gone, e_all.at[:, pl.ds(0, n_sp - 1 - s)], e_ssem.at[0]))
     both[core] = both[core] * nout[...]
@@ -519,6 +613,12 @@
                 pltpu.VMEM((2, rows // 2, width), F32),
                 pltpu.VMEM((rows // 2, width), F32),
                 pltpu.VMEM((n_tp, 8, LANES), F32),
+                pltpu.VMEM((n_chip, 2 * state, LANES), BF16),
+                pltpu.VMEM((n_tp, n_chip // 2, 2 * state, LANES), BF16),
+                pltpu.VMEM((n_tp - 2, 2 * lanes, n_chip // 2 * LANES), BF16),
+                pltpu.VMEM((2, rows // 2, LANES), BF16),
+                pltpu.VMEM((4, lanes), F32),
+                pltpu.VMEM((n_tp, 4, lanes), F32),
                 pltpu.VMEM((4, width, state), F32),
                 pltpu.VMEM((mine, d_model), BF16),
                 pltpu.VMEM((1, d_model), F32),
@@ -533,6 +633,8 @@
                 dma((1 + (n_chip - 1) * n_blk,)),
                 dma((2,)),
                 dma((4,)),
+                dma((2,)),
+                dma((2,)),
                 pltpu.SemaphoreType.REGULAR((3,)),
             ],
             compiler_params=pltpu.CompilerParams(collective_id=0, has_side_effects=True),

time: 17.8 us -> 17.5 us (0.983)
  Pallas kernels: 17 us -> 16.6 us
    pallas_call x1, Pallas kernels: 17 us -> 16.6 us  [on_device(): pl.pallas_call(functools.partial(layer, n_sp, n_tp, state, group), out_sh...]
where the time goes in v6:
time: 17.5 us; the launch traced here: 17.3 us
  Pallas kernels  16.6 us (95%)
  local copies, waits for them, and re-layouts  0.68 us (4%)
    pallas_call x1, Pallas kernels, on_device(): pl.pallas_call(functools.partial(layer, n_sp, n_tp, state, group), out_sh...  16.6 us
    unnamed x1, local copies, waits for them, and re-layouts  0.68 us

profile of v6, /device:TPU:24, one launch (start us, length us, event | category | flops | bytes accessed | tf_op | source)
XLA Modules:
  0.0 17.3 jit_solution(373583043679615960)
XLA Ops:
  0.0 16.6 %shard_map.118 = bf16[192,512]{1,0:T(8,128)(2,1)S(1)} custom-call(bf16[48,2048]{1,0:T(8,128)(2,1)} %tok_h.1, f32[1,2048]{1,0:T(1,128)} %bitcast.15, f32[32,64]{1,0:T(8,128)} %dlog_h.1, f32[32,64]{1,0:T(8,128)} %phase_h.1, f32[512,64]{1,0:T(8,128)} %bitcast.11, f32[512,64]{1,0:T(8,128)} %bitcast.12, f32[512,64]{1,0:T(8,128)} %bitcast.13, f32[512,64]{1,0:T(8,128)} %bitcast.14, ...), custom_call_target="tpu_custom_call" | custom-call | tf_op jit(solution)/shard_map/pallas_call | solution.py:586
  16.6 0.7 %copy.14 = bf16[192,512]{1,0:T(8,128)(2,1)} copy(bf16[192,512]{1,0:T(8,128)(2,1)S(1)} %shard_map.118) | data formatting | bytes 393216

commit v7 on v6

--- a/solution.py
+++ b/solution.py
@@ -44,9 +44,9 @@
     tok_h, nin_h, dlog_h, phase_h, bre_h, bim_h, cre_h, cim_h, skip_h, wv_h, wg_h, nout_h,
     out,
     nsend, urecv, rows_a, rows_p, t1r, t1i, t2r, t2i, bs, cs, wbuf, xbuf, wsum, ylocal,
-    e_send, e_all, l_ref, zst, zbuf, w, acc, both, swapped, sq_all, ct, xct, xcs, yst, lh, xlh,
+    e_send, e_all, l_ref, zst, zbuf, w, acc, both, swapped, sq_all, ct, xct, xcs, yst, lam, xlam, begin, xbegin,
     bc, tok, nin, ap, sn,
-    load_sem, a_send, a_recv, e_ssem, e_rsem, z_send, z_recv, w_sem, q_sem, c_sem, h_sem, met,
+    load_sem, a_recv, e_ssem, e_rsem, z_recv, w_sem, q_sem, x_sem, met,
 ):
     sp, tp = lax.axis_index("sp"), lax.axis_index("tp")
     mine, d_model = tok.shape
@@ -122,7 +122,7 @@
     def enter():
         pl.when(known > 0)(lambda: pl.semaphore_wait(barrier, known))
         below(lambda j, c: tell(met.at[jnp.where(sp - j > half, 1, 0)], "sp")(j, c))
-        lax.fori_loop(0, jnp.where(last, tp, 0), tell(met.at[2], "tp"), 0)
+        lax.fori_loop(0, jnp.where(last, tp, 0), tell(met.at[0], "tp"), 0)
 
     pl.when(last)(enter)
     loaded(0, 1)
@@ -136,11 +136,11 @@
             nsend[j, blk] = normed[:, at : at + LANES]
 
     pl.when(jnp.logical_not(last))(enter)
-    pl.when(last & (tp < n_tp - 1))(lambda: pl.semaphore_wait(met.at[2], n_tp - 1 - tp))
+    pl.when(last & (tp < n_tp - 1))(lambda: pl.semaphore_wait(met.at[0], n_tp - 1 - tp))
 
 
     def scatter(j, blk, at):
-        remote(nsend.at[j, blk], urecv.at[tp, blk], a_send.at[0], a_recv.at[at], {"tp": j}).start()
+        remote(nsend.at[j, blk], urecv.at[tp, blk], load_sem.at[0], a_recv.at[at], {"tp": j}).start()
 
     for blk in range(n_blk):
         for k in range(1, n_chip):
@@ -251,11 +251,13 @@
 
     @pl.when(sp > 0)
     def _():
+        lam[...] = l_ref[early, 2:4]
         across(
             lambda h, j: remote(
-                ct.at[pl.ds(h * half_chips, half_chips)], xct.at[tp], c_sem.at[0], c_sem.at[1], {"tp": j}
+                ct.at[pl.ds(h * half_chips, half_chips)], xct.at[tp], load_sem.at[2], x_sem.at[0], {"tp": j}
             ).start()
         )
+        across(lambda h, j: remote(lam, xlam.at[tp], load_sem.at[3], x_sem.at[1], {"tp": j}).start())
 
     lower = (
         lax.broadcasted_iota(jnp.int32, (span, span), 0)
@@ -263,7 +265,7 @@
     ).astype(BF16)
 
     def landed(ref, sem):
-        remote(ref, ref, a_send.at[0], sem, {"tp": partner}).wait_recv()
+        remote(ref, ref, load_sem.at[0], sem, {"tp": partner}).wait_recv()
 
     def gone(ref, sem):
         remote(ref, ref, sem, a_recv.at[0], {"tp": partner}).wait_send()
@@ -336,7 +338,7 @@
         if y is None or blk != early:
             cross(blk, zst.at[:, blk])
         remote(
-            zst.at[1 - core, blk], zbuf.at[tp, blk], z_send.at[0], z_recv.at[0], {"tp": partner}
+            zst.at[1 - core, blk], zbuf.at[tp, blk], load_sem.at[1], z_recv.at[0], {"tp": partner}
         ).start()
 
     def half_of(c):
@@ -347,7 +349,7 @@
         for k in range(1, n_chip):
             for h in (core, 1 - core):
                 remote(
-                    src.at[h], zbuf.at[tp, blk], z_send.at[0], z_recv.at[1 + (k - 1) * n_blk + blk],
+                    src.at[h], zbuf.at[tp, blk], load_sem.at[1], z_recv.at[1 + (k - 1) * n_blk + blk],
                     {"tp": 2 * lax.rem(chip + k, n_chip) + h},
                 ).start()
 
@@ -399,11 +401,14 @@
         for blk in range(n_blk + 2):
             if blk < n_blk:
                 take(blk)
+            if blk == n_blk - 1:
+                give(blk)
+                post(blk)
             if 1 <= blk <= n_blk:
                 scan(blk - 1)
             if 2 <= blk:
                 readout(blk - 2)
-            if blk < n_blk:
+            if blk < n_blk - 1:
                 give(blk)
                 post(blk)
             if blk - 2 == early:
@@ -427,8 +432,8 @@
         hr, hi = lax.fori_loop(0, sp, join, (nil, nil))
         hr, hi = cmul(hr, hi, l_ref[blk, 2:3], l_ref[blk, 3:4])
         if blk == early:
-            lh[...] = jnp.concatenate([l_ref[blk, 2:4], hr, hi], axis=0)
-            across(lambda h, j: remote(lh, xlh.at[tp], h_sem.at[0], h_sem.at[1], {"tp": j}).start())
+            begin[...] = jnp.concatenate([hr, hi], axis=0).astype(BF16)
+            across(lambda h, j: remote(begin, xbegin.at[tp], load_sem.at[4], x_sem.at[2], {"tp": j}).start())
         xr, xi = cmul(hr, hi, t2r[:, cut], t2i[:, cut])
         x = jnp.concatenate([xr.astype(BF16), xi.astype(BF16)], axis=1)
         finish(blk, jnp.dot(x, cs[blk], preferred_element_type=F32))
@@ -441,7 +446,8 @@
 
     @pl.when(sp > 0)
     def _():
-        landed(xct.at[pl.ds(0, n_tp - 2)], c_sem.at[1])
+        landed(xct.at[pl.ds(0, n_tp - 2)], x_sem.at[0])
+        landed(xlam.at[pl.ds(0, n_tp - 2)], x_sem.at[1])
         for k in range(1, n_chip):
             for h in range(2):
                 j = 2 * lax.rem(chip + n_chip - k, n_chip) + h
@@ -450,11 +456,14 @@
 
     def correct(k, c2):
         if k == 1:
-            landed(xlh.at[pl.ds(0, n_tp - 2)], h_sem.at[1])
+            landed(xbegin.at[pl.ds(0, n_tp - 2)], x_sem.at[2])
         fixed = []
         for h in range(2):
             j = c2 + h
-            lr, li, pr, pi = (jnp.broadcast_to(xlh[j, i : i + 1], (8, lanes)) for i in range(4))
+            first = xbegin[j].astype(F32)
+            lr, li, pr, pi = (
+                jnp.broadcast_to(part[i : i + 1], (8, lanes)) for part in (xlam[j], first) for i in range(2)
+            )
             row = lax.broadcasted_iota(jnp.int32, (8, lanes), 0)
             for bit in range(3):
                 on = lax.rem(row // (1 << bit), 2) == 1
@@ -526,7 +535,7 @@
         for blk in range(n_blk):
             piece = square[:, blk * LANES : (blk + 1) * LANES]
             part = piece if part is None else part + piece
-    remote(both.at[1 - core], swapped, q_sem.at[2], q_sem.at[3], {"tp": partner}).start()
+    remote(both.at[1 - core], swapped, q_sem.at[1], q_sem.at[2], {"tp": partner}).start()
     sums = jnp.sum(part, axis=1, keepdims=True)
     lane = lax.broadcasted_iota(jnp.int32, (8, LANES), 1)
     total = jnp.zeros((8, LANES), F32)
@@ -535,22 +544,23 @@
     sq_all[tp] = total
     for k in range(1, n_tp):
         j = lax.rem(tp + n_tp - k, n_tp)
-        remote(sq_all.at[tp], sq_all.at[tp], q_sem.at[0], q_sem.at[1], {"tp": j}).start()
-    gone(nsend.at[pl.ds(0, n_tp - 1)], a_send.at[0])
-    gone(zbuf.at[pl.ds(0, n_tp - 1)], z_send.at[0])
+        remote(sq_all.at[tp], sq_all.at[tp], load_sem.at[5], q_sem.at[0], {"tp": j}).start()
+    gone(nsend.at[pl.ds(0, n_tp - 1)], load_sem.at[0])
+    gone(zbuf.at[pl.ds(0, n_tp - 1)], load_sem.at[1])
     gone(w.at[core], w_sem.at[0])
 
     @pl.when(sp > 0)
     def _():
-        gone(xct.at[pl.ds(0, n_tp - 2)], c_sem.at[0])
-        gone(xlh.at[pl.ds(0, n_tp - 2)], h_sem.at[0])
+        gone(xct.at[pl.ds(0, n_tp - 2)], load_sem.at[2])
+        gone(xlam.at[pl.ds(0, n_tp - 2)], load_sem.at[3])
+        gone(xbegin.at[pl.ds(0, n_tp - 2)], load_sem.at[4])
 
     for s in range(n_sp - 1):
         pl.when(sp == s)(functools.partial(gone, e_all.at[:, pl.ds(0, n_sp - 1 - s)], e_ssem.at[0]))
     both[core] = both[core] * nout[...]
-    landed(swapped, q_sem.at[3])
+    landed(swapped, q_sem.at[2])
     swapped[...] = swapped[...] * nout[...]
-    landed(sq_all.at[pl.ds(0, n_tp - 1)], q_sem.at[1])
+    landed(sq_all.at[pl.ds(0, n_tp - 1)], q_sem.at[0])
     for h in (core, 1 - core):
         total = sq_all[h]
         for c in range(1, n_chip):
@@ -561,8 +571,8 @@
         at = pl.ds(pl.multiple_of(h * half_rows, half_rows), half_rows)
         out[at, :] = (gated * column).astype(BF16)
 
-    gone(sq_all.at[pl.ds(0, n_tp - 1)], q_sem.at[0])
-    gone(swapped, q_sem.at[2])
+    gone(sq_all.at[pl.ds(0, n_tp - 1)], load_sem.at[5])
+    gone(swapped, q_sem.at[1])
 
 
 def solution(mesh):
@@ -617,25 +627,24 @@
                 pltpu.VMEM((n_tp, n_chip // 2, 2 * state, LANES), BF16),
                 pltpu.VMEM((n_tp - 2, 2 * lanes, n_chip // 2 * LANES), BF16),
                 pltpu.VMEM((2, rows // 2, LANES), BF16),
-                pltpu.VMEM((4, lanes), F32),
-                pltpu.VMEM((n_tp, 4, lanes), F32),
+                pltpu.VMEM((2, lanes), F32),
+                pltpu.VMEM((n_tp, 2, lanes), F32),
+                pltpu.VMEM((2, lanes), BF16),
+                pltpu.VMEM((n_tp, 2, lanes), BF16),
                 pltpu.VMEM((4, width, state), F32),
                 pltpu.VMEM((mine, d_model), BF16),
                 pltpu.VMEM((1, d_model), F32),
                 pltpu.VMEM((2, groups, state), F32),
                 pltpu.VMEM((2, 1, width), F32),
                 dma((6,)),
-                dma((1,)),
                 dma((1 + (n_chip - 1) * n_blk,)),
                 dma((1,)),
                 dma((n_blk,)),
-                dma((1,)),
                 dma((1 + (n_chip - 1) * n_blk,)),
                 dma((2,)),
-                dma((4,)),
-                dma((2,)),
-                dma((2,)),
-                pltpu.SemaphoreType.REGULAR((3,)),
+                dma((3,)),
+                dma((3,)),
+                pltpu.SemaphoreType.REGULAR((2,)),
             ],
             compiler_params=pltpu.CompilerParams(collective_id=0, has_side_effects=True),
         )(

time: 17.5 us -> 17.3 us (0.989)
  Pallas kernels: 16.6 us -> 16.4 us
where the time goes in v7:
time: 17.3 us; the launch traced here: 17.1 us
  Pallas kernels  16.4 us (95%)
  local copies, waits for them, and re-layouts  0.68 us (4%)
    pallas_call x1, Pallas kernels, on_device(): pl.pallas_call(functools.partial(layer, n_sp, n_tp, state, group), out_sh...  16.4 us
    unnamed x1, local copies, waits for them, and re-layouts  0.68 us

profile of v7, /device:TPU:24, one launch (start us, length us, event | category | flops | bytes accessed | tf_op | source)
XLA Modules:
  0.0 17.1 jit_solution(7861569760066576139)
XLA Ops:
  0.0 16.4 %shard_map.118 = bf16[192,512]{1,0:T(8,128)(2,1)S(1)} custom-call(bf16[48,2048]{1,0:T(8,128)(2,1)} %tok_h.1, f32[1,2048]{1,0:T(1,128)} %bitcast.15, f32[32,64]{1,0:T(8,128)} %dlog_h.1, f32[32,64]{1,0:T(8,128)} %phase_h.1, f32[512,64]{1,0:T(8,128)} %bitcast.11, f32[512,64]{1,0:T(8,128)} %bitcast.12, f32[512,64]{1,0:T(8,128)} %bitcast.13, f32[512,64]{1,0:T(8,128)} %bitcast.14, ...), custom_call_target="tpu_custom_call" | custom-call | tf_op jit(solution)/shard_map/pallas_call | solution.py:596
  16.4 0.7 %copy.14 = bf16[192,512]{1,0:T(8,128)(2,1)} copy(bf16[192,512]{1,0:T(8,128)(2,1)S(1)} %shard_map.118) | data formatting | bytes 393216

commit v8 on v7

--- a/solution.py
+++ b/solution.py
@@ -62,7 +62,7 @@
     span = 2 * mine
     pair = 2 if n_sp % 2 == 0 else 1
     sp_b = lax.rem(sp, pair)
-    early = 0
+    n_early = min(2, n_blk)
     half_chips = n_chip // 2
 
     parts = [pl.ds(i * width, width) for i in range(n_tp)]
@@ -241,23 +241,36 @@
             if c:
                 c_r, c_i = cmul(c_r, c_i, *spread)
             turned = jnp.concatenate([c_r, -c_i], axis=1).T
-            if blk == early:
-                ct[c] = turned.astype(BF16)
+            if blk < n_early:
+                ct[blk, c] = turned.astype(BF16)
             widen(cs.at[blk], turned, c)
     def across(start):
         for k in range(1, n_chip):
             for h in range(2):
                 start(h, 2 * lax.rem(chip + k, n_chip) + h)
 
+    def slot(k, h, b):
+        return (k - 1) * (1 + n_early) + (n_early if h else b)
+
+    def share(b):
+        lam[b] = l_ref[b, 2:4]
+        across(
+            lambda h, j: remote(
+                ct.at[b, pl.ds(h * half_chips, half_chips)], xct.at[tp * n_early + b], load_sem.at[2], x_sem.at[0],
+                {"tp": j},
+            ).start()
+        )
+        across(
+            lambda h, j: remote(
+                lam.at[b], xlam.at[tp * n_early + b], load_sem.at[3], x_sem.at[1], {"tp": j}
+            ).start()
+        )
+
     @pl.when(sp > 0)
     def _():
-        lam[...] = l_ref[early, 2:4]
-        across(
-            lambda h, j: remote(
-                ct.at[pl.ds(h * half_chips, half_chips)], xct.at[tp], load_sem.at[2], x_sem.at[0], {"tp": j}
-            ).start()
-        )
-        across(lambda h, j: remote(lam, xlam.at[tp], load_sem.at[3], x_sem.at[1], {"tp": j}).start())
+        share(0)
+        for b in range(1, n_early):
+            pl.when(core == 0)(functools.partial(share, b))
 
     lower = (
         lax.broadcasted_iota(jnp.int32, (span, span), 0)
@@ -335,8 +348,10 @@
                 v = v + y[:, c * LANES : (c + 1) * LANES]
             top, to = half_of(c)
             zst[top, blk, to] = jax.nn.gelu(v).astype(BF16)
-        if y is None or blk != early:
+        if y is None or blk >= n_early:
             cross(blk, zst.at[:, blk])
+        elif blk:
+            pl.when(core == 1)(lambda: cross(blk, zst.at[:, blk]))
         remote(
             zst.at[1 - core, blk], zbuf.at[tp, blk], load_sem.at[1], z_recv.at[0], {"tp": partner}
         ).start()
@@ -344,6 +359,12 @@
     def half_of(c):
         top = c * span // half_rows
         return top, slice(c * span - top * half_rows, (c + 1) * span - top * half_rows)
+
+    def ahead(b):
+        for c in range(n_chip):
+            top, to = half_of(c)
+            yst[b, top, to] = ylocal[b][c * span : (c + 1) * span].astype(BF16)
+        cross(b, yst.at[b])
 
     def cross(blk, src):
         for k in range(1, n_chip):
@@ -411,11 +432,10 @@
             if blk < n_blk - 1:
                 give(blk)
                 post(blk)
-            if blk - 2 == early:
-                for c in range(n_chip):
-                    top, to = half_of(c)
-                    yst[top, to] = ylocal[early][c * span : (c + 1) * span].astype(BF16)
-                cross(early, yst)
+            if blk - 2 == 0:
+                ahead(0)
+            elif 0 < blk - 2 < n_early:
+                pl.when(core == 0)(functools.partial(ahead, blk - 2))
 
     def after(blk):
         cut = slice(blk * lanes, (blk + 1) * lanes)
@@ -431,9 +451,19 @@
         nil = jnp.zeros((1, lanes), F32)
         hr, hi = lax.fori_loop(0, sp, join, (nil, nil))
         hr, hi = cmul(hr, hi, l_ref[blk, 2:3], l_ref[blk, 3:4])
-        if blk == early:
-            begin[...] = jnp.concatenate([hr, hi], axis=0).astype(BF16)
-            across(lambda h, j: remote(begin, xbegin.at[tp], load_sem.at[4], x_sem.at[2], {"tp": j}).start())
+
+        def tell_begin():
+            begin[blk] = jnp.concatenate([hr, hi], axis=0).astype(BF16)
+            across(
+                lambda h, j: remote(
+                    begin.at[blk], xbegin.at[tp * n_early + blk], load_sem.at[4], x_sem.at[2 + blk], {"tp": j}
+                ).start()
+            )
+
+        if blk == 0:
+            tell_begin()
+        elif blk < n_early:
+            pl.when(core == 0)(tell_begin)
         xr, xi = cmul(hr, hi, t2r[:, cut], t2i[:, cut])
         x = jnp.concatenate([xr.astype(BF16), xi.astype(BF16)], axis=1)
         finish(blk, jnp.dot(x, cs[blk], preferred_element_type=F32))
@@ -446,20 +476,22 @@
 
     @pl.when(sp > 0)
     def _():
-        landed(xct.at[pl.ds(0, n_tp - 2)], x_sem.at[0])
-        landed(xlam.at[pl.ds(0, n_tp - 2)], x_sem.at[1])
+        for ref, sem in ((xct, 0), (xlam, 1)):
+            landed(ref.at[pl.ds(0, (n_chip - 1) * (1 + n_early))], x_sem.at[sem])
         for k in range(1, n_chip):
             for h in range(2):
                 j = 2 * lax.rem(chip + n_chip - k, n_chip) + h
-                for c in range(half_chips):
-                    widen(xcs.at[2 * (k - 1) + h], xct[j, c].astype(F32), c)
-
-    def correct(k, c2):
+                for b in range(1 if h else n_early):
+                    for c in range(half_chips):
+                        widen(xcs.at[slot(k, h, b)], xct[j * n_early + b, c].astype(F32), c)
+
+    def correct(k, c2, b):
+        heads = range(1 if b else 2)
         if k == 1:
-            landed(xbegin.at[pl.ds(0, n_tp - 2)], x_sem.at[2])
+            landed(xbegin.at[pl.ds(0, (n_chip - 1) * len(heads))], x_sem.at[2 + b])
         fixed = []
-        for h in range(2):
-            j = c2 + h
+        for h in heads:
+            j = (c2 + h) * n_early + b
             first = xbegin[j].astype(F32)
             lr, li, pr, pi = (
                 jnp.broadcast_to(part[i : i + 1], (8, lanes)) for part in (xlam[j], first) for i in range(2)
@@ -477,13 +509,13 @@
             x = jnp.concatenate(
                 [jnp.concatenate([p[i] for p in pieces], axis=0).astype(BF16) for i in range(2)], axis=1
             )
-            fixed.append(jnp.dot(x, xcs[2 * (k - 1) + h], preferred_element_type=F32))
-        held = [zbuf[c2 + h, early].astype(F32) for h in range(2)]
-        for h in range(2):
+            fixed.append(jnp.dot(x, xcs[slot(k, h, b)], preferred_element_type=F32))
+        held = [zbuf[c2 + h, b].astype(F32) for h in heads]
+        for h in heads:
             y = jnp.concatenate([fixed[h][:, c * LANES : (c + 1) * LANES] for c in range(half_chips)], axis=0)
             held[h] = jax.nn.gelu(held[h] + y).astype(BF16)
-        for h in range(2):
-            zbuf[c2 + h, early] = held[h]
+        for h in heads:
+            zbuf[c2 + h, b] = held[h]
 
     loaded(5)
 
@@ -521,8 +553,8 @@
         for k in range(1, n_chip):
             c2 = 2 * lax.rem(chip + n_chip - k, n_chip)
             landed(zbuf.at[pl.ds(c2, 2), blk], z_recv.at[1 + (k - 1) * n_blk + blk])
-            if blk == early:
-                pl.when(sp > 0)(functools.partial(correct, k, c2))
+            if blk < n_early:
+                pl.when(sp > 0)(functools.partial(correct, k, c2, blk))
             new = products(*(project(zbuf, c2 + h, c2 + h, [blk]) for h in range(2)))
             if blk < n_blk - 1 or k < n_chip - 1:
                 add(new)
@@ -551,9 +583,12 @@
 
     @pl.when(sp > 0)
     def _():
-        gone(xct.at[pl.ds(0, n_tp - 2)], load_sem.at[2])
-        gone(xlam.at[pl.ds(0, n_tp - 2)], load_sem.at[3])
-        gone(xbegin.at[pl.ds(0, n_tp - 2)], load_sem.at[4])
+        for h in range(2):
+
+            @pl.when(core == h)
+            def _(count=(n_tp - 2) * (1 if h else n_early)):
+                for ref, sem in ((xct, 2), (xlam, 3), (xbegin, 4)):
+                    gone(ref.at[pl.ds(0, count)], load_sem.at[sem])
 
     for s in range(n_sp - 1):
         pl.when(sp == s)(functools.partial(gone, e_all.at[:, pl.ds(0, n_sp - 1 - s)], e_ssem.at[0]))
@@ -589,6 +624,7 @@
         lanes = LANES // group * state
         entries = groups * state
         n_chip = n_tp // 2
+        n_early = min(2, n_blk)
         span = 2 * mine
         vmem = pl.BlockSpec(memory_space=pltpu.VMEM)
         hbm = pl.BlockSpec(memory_space=pl.ANY)
@@ -623,14 +659,14 @@
                 pltpu.VMEM((2, rows // 2, width), F32),
                 pltpu.VMEM((rows // 2, width), F32),
                 pltpu.VMEM((n_tp, 8, LANES), F32),
-                pltpu.VMEM((n_chip, 2 * state, LANES), BF16),
-                pltpu.VMEM((n_tp, n_chip // 2, 2 * state, LANES), BF16),
-                pltpu.VMEM((n_tp - 2, 2 * lanes, n_chip // 2 * LANES), BF16),
-                pltpu.VMEM((2, rows // 2, LANES), BF16),
-                pltpu.VMEM((2, lanes), F32),
-                pltpu.VMEM((n_tp, 2, lanes), F32),
-                pltpu.VMEM((2, lanes), BF16),
-                pltpu.VMEM((n_tp, 2, lanes), BF16),
+                pltpu.VMEM((n_early, n_chip, 2 * state, LANES), BF16),
+                pltpu.VMEM((n_tp * n_early, n_chip // 2, 2 * state, LANES), BF16),
+                pltpu.VMEM(((n_chip - 1) * (1 + n_early), 2 * lanes, n_chip // 2 * LANES), BF16),
+                pltpu.VMEM((n_early, 2, rows // 2, LANES), BF16),
+                pltpu.VMEM((n_early, 2, lanes), F32),
+                pltpu.VMEM((n_tp * n_early, 2, lanes), F32),
+                pltpu.VMEM((n_early, 2, lanes), BF16),
+                pltpu.VMEM((n_tp * n_early, 2, lanes), BF16),
                 pltpu.VMEM((4, width, state), F32),
                 pltpu.VMEM((mine, d_model), BF16),
                 pltpu.VMEM((1, d_model), F32),
@@ -643,7 +679,7 @@
                 dma((1 + (n_chip - 1) * n_blk,)),
                 dma((2,)),
                 dma((3,)),
-                dma((3,)),
+                dma((2 + n_early,)),
                 pltpu.SemaphoreType.REGULAR((2,)),
             ],
             compiler_params=pltpu.CompilerParams(collective_id=0, has_side_effects=True),

time: 17.3 us -> 17 us (0.983)
  the two profiles are of different devices: /device:TPU:24 before, /device:TPU:0 now
where the time goes in v8:
time: 17 us; the launch traced here: 16.9 us
  Pallas kernels  16.2 us (95%)
  local copies, waits for them, and re-layouts  0.68 us (4%)
    pallas_call x1, Pallas kernels, on_device(): pl.pallas_call(functools.partial(layer, n_sp, n_tp, state, group), out_sh...  16.2 us
    unnamed x1, local copies, waits for them, and re-layouts  0.68 us

profile of v8, /device:TPU:0, one launch (start us, length us, event | category | flops | bytes accessed | tf_op | source)
XLA Modules:
  0.0 16.9 jit_solution(7860191170692463794)
XLA Ops:
  0.0 16.2 %shard_map.118 = bf16[192,512]{1,0:T(8,128)(2,1)S(1)} custom-call(bf16[48,2048]{1,0:T(8,128)(2,1)} %tok_h.1, f32[1,2048]{1,0:T(1,128)} %bitcast.15, f32[32,64]{1,0:T(8,128)} %dlog_h.1, f32[32,64]{1,0:T(8,128)} %phase_h.1, f32[512,64]{1,0:T(8,128)} %bitcast.11, f32[512,64]{1,0:T(8,128)} %bitcast.12, f32[512,64]{1,0:T(8,128)} %bitcast.13, f32[512,64]{1,0:T(8,128)} %bitcast.14, ...), custom_call_target="tpu_custom_call" | custom-call | tf_op jit(solution)/shard_map/pallas_call | solution.py:632
  16.2 0.7 %copy.14 = bf16[192,512]{1,0:T(8,128)(2,1)} copy(bf16[192,512]{1,0:T(8,128)(2,1)S(1)} %shard_map.118) | data formatting | bytes 393216

commit v9 on v8

--- a/solution.py
+++ b/solution.py
@@ -348,7 +348,10 @@
                 v = v + y[:, c * LANES : (c + 1) * LANES]
             top, to = half_of(c)
             zst[top, blk, to] = jax.nn.gelu(v).astype(BF16)
-        if y is None or blk >= n_early:
+        if y is None:
+            for h, b in [(0, blk)] + [(1, b) for b in (blk - 1, blk) if 0 <= b and (b < blk or blk == n_blk - 1)]:
+                cross(b, zst.at[:, b], (h,))
+        elif blk >= n_early:
             cross(blk, zst.at[:, blk])
         elif blk:
             pl.when(core == 1)(lambda: cross(blk, zst.at[:, blk]))
@@ -366,9 +369,9 @@
             yst[b, top, to] = ylocal[b][c * span : (c + 1) * span].astype(BF16)
         cross(b, yst.at[b])
 
-    def cross(blk, src):
+    def cross(blk, src, heads=(core, 1 - core)):
         for k in range(1, n_chip):
-            for h in (core, 1 - core):
+            for h in heads:
                 remote(
                     src.at[h], zbuf.at[tp, blk], load_sem.at[1], z_recv.at[1 + (k - 1) * n_blk + blk],
                     {"tp": 2 * lax.rem(chip + k, n_chip) + h},
@@ -420,18 +423,25 @@
     @pl.when(sp > 0)
     def _():
         for blk in range(n_blk + 2):
-            if blk < n_blk:
-                take(blk)
+            def region(soon, blk=blk):
+                if blk < n_blk:
+                    take(blk)
+                if soon:
+                    give(blk)
+                    post(blk)
+                if 1 <= blk <= n_blk:
+                    scan(blk - 1)
+                if 2 <= blk:
+                    readout(blk - 2)
+                if blk < n_blk and not soon:
+                    give(blk)
+                    post(blk)
+
             if blk == n_blk - 1:
-                give(blk)
-                post(blk)
-            if 1 <= blk <= n_blk:
-                scan(blk - 1)
-            if 2 <= blk:
-                readout(blk - 2)
-            if blk < n_blk - 1:
-                give(blk)
-                post(blk)
+                pl.when(core == 0)(functools.partial(region, True))
+                pl.when(core == 1)(functools.partial(region, False))
+            else:
+                region(False)
             if blk - 2 == 0:
                 ahead(0)
             elif 0 < blk - 2 < n_early:

time: 17 us -> 16.9 us (level)
  the two profiles are of different devices: /device:TPU:0 before, /device:TPU:24 now
where the time goes in v9:
time: 16.9 us; the launch traced here: 16.7 us
  Pallas kernels  16 us (95%)
  local copies, waits for them, and re-layouts  0.68 us (4%)
    pallas_call x1, Pallas kernels, on_device(): pl.pallas_call(functools.partial(layer, n_sp, n_tp, state, group), out_sh...  16 us
    unnamed x1, local copies, waits for them, and re-layouts  0.68 us

profile of v9, /device:TPU:24, one launch (start us, length us, event | category | flops | bytes accessed | tf_op | source)
XLA Modules:
  0.0 16.7 jit_solution(8328965010533717785)
XLA Ops:
  0.0 16.0 %shard_map.118 = bf16[192,512]{1,0:T(8,128)(2,1)S(1)} custom-call(bf16[48,2048]{1,0:T(8,128)(2,1)} %tok_h.1, f32[1,2048]{1,0:T(1,128)} %bitcast.15, f32[32,64]{1,0:T(8,128)} %dlog_h.1, f32[32,64]{1,0:T(8,128)} %phase_h.1, f32[512,64]{1,0:T(8,128)} %bitcast.11, f32[512,64]{1,0:T(8,128)} %bitcast.12, f32[512,64]{1,0:T(8,128)} %bitcast.13, f32[512,64]{1,0:T(8,128)} %bitcast.14, ...), custom_call_target="tpu_custom_call" | custom-call | tf_op jit(solution)/shard_map/pallas_call | solution.py:642
  16.0 0.7 %copy.14 = bf16[192,512]{1,0:T(8,128)(2,1)} copy(bf16[192,512]{1,0:T(8,128)(2,1)S(1)} %shard_map.118) | data formatting | bytes 393216

commit v10 on v9

--- a/solution.py
+++ b/solution.py
@@ -65,13 +65,13 @@
     n_early = min(2, n_blk)
     half_chips = n_chip // 2
 
-    parts = [pl.ds(i * width, width) for i in range(n_tp)]
+    parts = [pl.ds(i, 8) for i in range(0, mine, 8)]
 
     def load(i, *pairs):
         return [pltpu.make_async_copy(src, dst, load_sem.at[i]) for src, dst in pairs]
 
     loads = [
-        load(0, *((tok_h.at[:, part], tok.at[:, part]) for part in parts)),
+        load(0, *((tok_h.at[part], tok.at[part]) for part in parts)),
         load(1, (nin_h, nin)),
         load(2, (dlog_h, ap.at[0]), (phase_h, ap.at[1])),
         load(3, *((src, bc.at[i]) for i, src in enumerate((bre_h, bim_h, cre_h, cim_h)))),

time: 16.9 us -> 16.9 us (level)
  no operation moved by 1% of the time
where the time goes in v10:
time: 16.9 us; the launch traced here: 16.6 us
  Pallas kernels  15.9 us (94%)
  local copies, waits for them, and re-layouts  0.68 us (4%)
    pallas_call x1, Pallas kernels, on_device(): pl.pallas_call(functools.partial(layer, n_sp, n_tp, state, group), out_sh...  15.9 us
    unnamed x1, local copies, waits for them, and re-layouts  0.68 us

profile of v10, /device:TPU:24, one launch (start us, length us, event | category | flops | bytes accessed | tf_op | source)
XLA Modules:
  0.0 16.6 jit_solution(15736392675162981873)
XLA Ops:
  0.0 15.9 %shard_map.118 = bf16[192,512]{1,0:T(8,128)(2,1)S(1)} custom-call(bf16[48,2048]{1,0:T(8,128)(2,1)} %tok_h.1, f32[1,2048]{1,0:T(1,128)} %bitcast.15, f32[32,64]{1,0:T(8,128)} %dlog_h.1, f32[32,64]{1,0:T(8,128)} %phase_h.1, f32[512,64]{1,0:T(8,128)} %bitcast.11, f32[512,64]{1,0:T(8,128)} %bitcast.12, f32[512,64]{1,0:T(8,128)} %bitcast.13, f32[512,64]{1,0:T(8,128)} %bitcast.14, ...), custom_call_target="tpu_custom_call" | custom-call | tf_op jit(solution)/shard_map/pallas_call | solution.py:642
  15.9 0.7 %copy.14 = bf16[192,512]{1,0:T(8,128)(2,1)} copy(bf16[192,512]{1,0:T(8,128)(2,1)S(1)} %shard_map.118) | data formatting | bytes 393216
